TPU v7x, 32 devices: a whole 2x2x4 slice. The times are simulated.
32 devices in a mesh: sp: 4 (over z), tp: 8 (over y, x, core).
Axes of the slice: x: 2, y: 2, z: 4, core: 2. Of those that a mesh axis runs over, the one named last changes fastest.
Arguments:
- target_rows: bfloat16 [768, 2048], P(('sp', 'tp')), may hold values from -6 to 6
- source_rows: bfloat16 [4096, 2048], P(('sp', 'tp')), may hold values from -6 to 6
- target_gain: float32 [2048], replicated, may hold values from 0.55 to 9
- source_gain: float32 [2048], replicated, may hold values from 0.55 to 9
- query_weight: bfloat16 [2048, 2048], P(None, 'tp'), may hold values from -0.125 to 0.125
- key_weight: bfloat16 [2048, 512], P('tp'), may hold values from -0.125 to 0.125
- value_weight: bfloat16 [2048, 512], P('tp'), may hold values from -0.125 to 0.125
- out_weight: bfloat16 [2048, 2048], P('tp'), may hold values from -0.125 to 0.125
- out_cotangent: bfloat16 [768, 2048], P(('sp', 'tp')), may hold values from -6 to 6
Outputs:
- target_grad: float32 [768, 2048], P(('sp', 'tp'))
- source_grad: float32 [4096, 2048], P(('sp', 'tp'))
- out_weight_grad: float32 [2048, 2048], P('tp')
All inputs are finite; a program needn't handle non-finite values.
Results may differ from a plain program's by a relative error of at most 0.03.
Values may be sent and summed in bfloat16 or wider, within the bound.
A program may use at most 64 MiB of HBM per device.

v0:
```python
import functools

import jax
import jax.numpy as jnp
from jax import lax
from jax.experimental import pallas as pl
from jax.experimental.pallas import tpu as pltpu
from jax.sharding import PartitionSpec as P

HEAD_DIM = 64
KV_HEADS = 8
EPSILON = 1e-06
MESH = pl.DeviceIdType.MESH


def normalize(matrix, gain_vector):
    widened = matrix.astype(jnp.float32)
    factor = lax.rsqrt(jnp.mean(widened * widened, axis=-1, keepdims=True) + EPSILON)
    return (widened * factor * gain_vector).astype(jnp.bfloat16)


def norm_back(matrix, gain_vector, upstream):
    widened = matrix.astype(jnp.float32)
    factor = lax.rsqrt(jnp.mean(widened * widened, axis=-1, keepdims=True) + EPSILON)
    weighted = upstream * gain_vector
    inner_sum = jnp.mean(weighted * widened, axis=-1, keepdims=True)
    return factor * weighted - widened * factor**3 * inner_sum


def exchange_kernel(kinds, sp_n, tp_n, *refs):
    count = len(kinds)
    ins, outs = refs[:count], refs[count : 2 * count]
    send_sems, recv_sems = refs[2 * count : 3 * count], refs[3 * count :]
    sp_me, tp_me = lax.axis_index("sp"), lax.axis_index("tp")
    sizes, places = {"sp": sp_n, "tp": tp_n}, {"sp": sp_me, "tp": tp_me}

    def address(axis, peer):
        return (peer, tp_me) if axis == "sp" else (sp_me, peer)

    axes = sorted({kind.split("_")[1] for kind in kinds})
    barrier = pltpu.get_barrier_semaphore()
    for axis in axes:
        for k in range(1, sizes[axis]):
            peer = lax.rem(places[axis] + k, sizes[axis])
            pl.semaphore_signal(barrier, inc=1, device_id=address(axis, peer), device_id_type=MESH)
    pl.semaphore_wait(barrier, sum(sizes[axis] - 1 for axis in axes))

    def copy(i, axis, source, slot, k, peer):
        return pltpu.make_async_remote_copy(
            src_ref=source,
            dst_ref=outs[i].at[slot],
            send_sem=send_sems[i].at[k],
            recv_sem=recv_sems[i].at[slot],
            device_id=address(axis, peer),
            device_id_type=MESH,
        )

    sent = []
    used = [0] * count

    def send(i, axis, source, target, recv, peer, keep=True):
        one = pltpu.make_async_remote_copy(
            src_ref=source,
            dst_ref=target,
            send_sem=send_sems[i].at[used[i]],
            recv_sem=recv_sems[i].at[recv],
            device_id=address(axis, peer),
            device_id_type=MESH,
        )
        used[i] += 1
        one.start()
        if keep:
            sent.append(one)
        return one

    def arrived(i, axis, target, recv):
        pltpu.make_async_remote_copy(
            src_ref=target,
            dst_ref=target,
            send_sem=send_sems[i].at[0],
            recv_sem=recv_sems[i].at[recv],
            device_id=address(axis, lax.rem(places[axis] + 1, sizes[axis])),
            device_id_type=MESH,
        ).wait_recv()

    square = tp_n == 8
    partner = tp_me + 1 - 2 * lax.rem(tp_me, 2)

    def across(index):
        return index + 2 - 4 * lax.rem(index // 2, 2)

    def along(index):
        return index + 4 - 8 * lax.rem(index // 4, 2)

    def relatives(index):
        if square:
            return [across(index), along(index)]
        return [lax.rem(index + 2 * k, tp_n) for k in range(1, tp_n // 2)]

    def forward(i, c, origin):
        chunks = ins[i].shape[0]
        piece, recv = outs[i].at[origin, c], origin * chunks + c
        arrived(i, "tp", piece, recv)
        send(i, "tp", piece, piece, recv, partner)
        return piece, recv

    line_sent = []
    depth = max([ins[i].shape[0] for i in range(count) if kinds[i] == "pair_tp"], default=0)
    for c in range(depth):
        for i, kind in enumerate(kinds):
            if kind == "pair_tp" and c < ins[i].shape[0]:
                chunks = ins[i].shape[0]
                for peer in relatives(tp_me) + [partner]:
                    piece = outs[i].at[tp_me, c]
                    send(i, "tp", ins[i].at[c], piece, tp_me * chunks + c, peer)
    for i, kind in enumerate(kinds):
        mode, axis = kind.split("_")
        n, me = sizes[axis], places[axis]
        if mode == "line":
            for step in (1, -1):
                inside = (me < n - 1) if step == 1 else (me > 0)
                for c in range(ins[i].shape[0]):
                    line_sent.append((i, inside, used[i], me, c))
                    recv = me * ins[i].shape[0] + c

                    @pl.when(inside)
                    def _():
                        piece = outs[i].at[me, c]
                        send(i, axis, ins[i].at[c], piece, recv, me + step, keep=False)
        elif mode != "pair":
            for k in range(1, n):
                peer = lax.rem(me + k, n)
                source = ins[i] if mode == "gather" else ins[i].at[peer]
                send(i, axis, source, outs[i].at[me], me, peer)
    for i, kind in enumerate(kinds):
        mode, axis = kind.split("_")
        me = places[axis]
        outs[i][me] = ins[i][me] if mode == "swap" else ins[i][...]

    def line_step(i, far, c):
        n, me = sp_n, sp_me
        chunks = ins[i].shape[0]
        for step in (1, -1):
            origin = me - step * far
            valid = (origin >= 0) if step == 1 else (origin <= n - 1)
            onward = (valid & (me < n - 1)) if step == 1 else (valid & (me > 0))

            @pl.when(valid)
            def _():
                arrived(i, "sp", outs[i].at[origin, c], origin * chunks + c)

            if far < n - 1:
                line_sent.append((i, onward, used[i], origin, c))

                @pl.when(onward)
                def _():
                    piece = outs[i].at[origin, c]
                    recv = origin * chunks + c
                    send(i, "sp", piece, piece, recv, me + step, keep=False)

    def pair_step(i, c):
        me = tp_me
        chunks = ins[i].shape[0]
        for order, origin in enumerate(relatives(me)):
            piece, recv = forward(i, c, origin)
            if square and order == (i + c) % 2:
                send(i, "tp", piece, piece, recv, along(me) if order == 0 else across(me))

    lines = [i for i in range(count) if kinds[i] == "line_sp"]
    pairs = [i for i in range(count) if kinds[i] == "pair_tp"]
    for turn in range(max(depth, sp_n - 1 if lines else 0)):
        for i in pairs:
            if turn < ins[i].shape[0]:
                pair_step(i, turn)
        for i in lines:
            if turn + 1 < sp_n:
                for c in range(ins[i].shape[0]):
                    line_step(i, turn + 1, c)
    if square:
        for c in range(depth):
            for i in pairs:
                if c < ins[i].shape[0]:
                    forward(i, c, across(along(tp_me)))
    for i, kind in enumerate(kinds):
        mode, axis = kind.split("_")
        n, me = sizes[axis], places[axis]
        if mode == "pair":
            chunks = ins[i].shape[0]
            others = relatives(partner) + ([across(along(partner))] if square else [])
            for origin in [partner] + others:
                for c in range(chunks):
                    arrived(i, axis, outs[i].at[origin, c], origin * chunks + c)
        elif mode != "line":
            for k in range(1, n):
                origin = lax.rem(me + n - k, n)
                arrived(i, axis, outs[i].at[origin], origin)
    for one in sent:
        one.wait_send()
    for i, happened, slot, origin, c in line_sent:

        @pl.when(happened)
        def _():
            pltpu.make_async_remote_copy(
                src_ref=outs[i].at[origin, c],
                dst_ref=outs[i].at[origin, c],
                send_sem=send_sems[i].at[slot],
                recv_sem=recv_sems[i].at[0],
                device_id=address("sp", lax.rem(sp_me + 1, sp_n)),
                device_id_type=MESH,
            ).wait_send()


def exchange(collective_id, *parts):
    sp_n, tp_n = lax.axis_size("sp"), lax.axis_size("tp")
    kinds = tuple(kind for kind, array in parts)
    arrays = [array for kind, array in parts]
    shapes, sends, recvs = [], [], []
    for kind, array in parts:
        mode, axis = kind.split("_")
        n = sp_n if axis == "sp" else tp_n
        shape = array.shape if mode == "swap" else (n,) + array.shape
        shapes.append(jax.ShapeDtypeStruct(shape, array.dtype))
        chunks = array.shape[0] if mode in ("pair", "line") else 1
        sends.append(pltpu.SemaphoreType.DMA(((2 * n + 8) * chunks,)))
        recvs.append(pltpu.SemaphoreType.DMA((n * chunks,)))
    return pl.pallas_call(
        functools.partial(exchange_kernel, kinds, sp_n, tp_n),
        out_shape=shapes,
        in_specs=[pl.BlockSpec(memory_space=pltpu.VMEM)] * len(parts),
        out_specs=[pl.BlockSpec(memory_space=pltpu.VMEM)] * len(parts),
        scratch_shapes=sends + recvs,
        compiler_params=pltpu.CompilerParams(
            collective_id=collective_id,
            has_side_effects=True,
            vmem_limit_bytes=56 * 1024 * 1024,
        ),
    )(*arrays)


def matmul(left, right):
    return jnp.dot(left, right, preferred_element_type=jnp.float32)


def einsum(text, left, right):
    return jnp.einsum(text, left, right, preferred_element_type=jnp.float32)


def body(
    target_rows,
    source_rows,
    target_gain,
    source_gain,
    query_weight,
    key_weight,
    value_weight,
    out_weight,
    out_cotangent,
):
    sp_n, tp_n = lax.axis_size("sp"), lax.axis_size("tp")
    width = target_rows.shape[1]
    local_width = query_weight.shape[1]
    local_heads = local_width // HEAD_DIM
    slot_heads = max(1, KV_HEADS // tp_n)
    copies = max(1, tp_n // KV_HEADS)
    per_slot = local_heads // slot_heads
    slot_width = slot_heads * HEAD_DIM
    score_scale = HEAD_DIM ** (-0.5)
    bf16 = jnp.bfloat16

    normed_t = normalize(target_rows, target_gain)
    normed_s = normalize(source_rows, source_gain)
    source_local = normed_s.shape[0]
    target_local = normed_t.shape[0]
    target_block = tp_n * target_local
    source_block = tp_n * source_local

    rows_in, cot_in = exchange(
        0,
        ("pair_tp", normed_t[None]),
        ("pair_tp", out_cotangent[None]),
    )
    queries = matmul(rows_in.reshape(target_block, width), query_weight).astype(bf16)
    d_attended = matmul(cot_in.reshape(target_block, width), out_weight.T).astype(bf16)
    halves = (2, key_weight.shape[0] // 2, key_weight.shape[1])
    split = (2, target_block // 2, local_width)
    key_full, value_full, all_queries, all_grads, cot_column = exchange(
        1,
        ("pair_tp", key_weight.reshape(halves)),
        ("pair_tp", value_weight.reshape(halves)),
        ("line_sp", queries.reshape(split)),
        ("line_sp", d_attended.reshape(split)),
        ("line_sp", out_cotangent[None]),
    )
    key_full = key_full.reshape(width, -1)
    value_full = value_full.reshape(width, -1)
    key_own = matmul(normed_s, key_full).astype(bf16)
    value_own = matmul(normed_s, value_full).astype(bf16)

    def to_slots(matrix):
        split = matrix.reshape(source_local, tp_n // copies, 1, slot_width)
        spread = jnp.broadcast_to(split, (source_local, tp_n // copies, copies, slot_width))
        return spread.reshape(source_local, tp_n, slot_width).transpose(1, 0, 2)

    slots = jnp.concatenate([to_slots(key_own), to_slots(value_own)], axis=2)
    (kv_block,) = exchange(2, ("swap_tp", slots))
    whole_rows = sp_n * target_block
    kv_block = kv_block.reshape(source_block, 2, slot_heads, HEAD_DIM)
    keys, values = kv_block[:, 0], kv_block[:, 1]
    head_shape = (whole_rows, slot_heads, per_slot, HEAD_DIM)
    query_view = all_queries.reshape(head_shape)
    grad_view = all_grads.reshape(head_shape)

    scores = einsum("tgqd,sgd->gqts", query_view, keys) * score_scale
    part_max = jnp.max(scores, axis=-1)
    weights = jnp.exp(scores - part_max[..., None])
    part_total = jnp.sum(weights, axis=-1)
    d_probs = einsum("tgqd,sgd->gqts", grad_view, values)
    part_delta = jnp.sum(weights * d_probs, axis=-1)
    part_sum = einsum("gqts,sgd->tgqd", weights.astype(bf16), values)
    stats = jnp.stack([part_max, part_total, part_delta]).reshape(3 * local_heads, whole_rows)
    (all_stats,) = exchange(3, ("gather_sp", stats))
    all_stats = all_stats.reshape(sp_n, 3, slot_heads, per_slot, whole_rows)
    row_max = jnp.max(all_stats[:, 0], axis=0)
    rescale = jnp.exp(all_stats[:, 0] - row_max)
    total = jnp.sum(all_stats[:, 1] * rescale, axis=0)
    delta = jnp.sum(all_stats[:, 2] * rescale, axis=0) / total
    local_scale = jnp.exp(part_max - row_max) / total

    attended_part = part_sum * local_scale.transpose(2, 0, 1)[..., None]
    attended_part = attended_part.reshape(sp_n, target_block, local_width).astype(bf16)
    probs = weights * local_scale[..., None]
    d_scores = (probs * (d_probs - delta[..., None])).astype(bf16)
    value_sum = einsum("gqts,tgqd->sgd", probs.astype(bf16), grad_view)
    key_sum = einsum("gqts,tgqd->sgd", d_scores, query_view) * score_scale
    d_query = einsum("gqts,sgd->tgqd", d_scores, keys) * score_scale
    d_query = d_query.reshape(sp_n, target_block, local_width).astype(bf16)
    grads = jnp.concatenate(
        [key_sum.reshape(source_block, slot_width), value_sum.reshape(source_block, slot_width)],
        axis=1,
    )
    grads = grads.reshape(tp_n, source_local, 2 * slot_width).astype(bf16)
    query_terms, attended_terms, grads_back, cot_all = exchange(
        4,
        ("swap_sp", d_query),
        ("swap_sp", attended_part),
        ("swap_tp", grads),
        ("pair_tp", cot_column.reshape(sp_n, target_local, width)),
    )
    query_grad = jnp.sum(query_terms.astype(jnp.float32), axis=0).astype(bf16)
    attended = jnp.sum(attended_terms.astype(jnp.float32), axis=0).astype(bf16)

    target_terms = matmul(query_grad, query_weight.T).astype(bf16)
    target_back, attended_all = exchange(
        5,
        ("swap_tp", target_terms.reshape(tp_n, target_local, width)),
        ("line_sp", attended.reshape(split)),
    )

    def from_slots(matrix):
        folded = matrix.reshape(tp_n // copies, copies, source_local, slot_width)
        folded = jnp.sum(folded.astype(jnp.float32), axis=1)
        return folded.transpose(1, 0, 2).reshape(source_local, -1).astype(bf16)

    key_grad = from_slots(grads_back[:, :, :slot_width])
    value_grad = from_slots(grads_back[:, :, slot_width:])
    d_normed_s = matmul(key_grad, key_full.T) + matmul(value_grad, value_full.T)
    source_grad = norm_back(source_rows, source_gain, d_normed_s)
    d_normed_t = jnp.sum(target_back.astype(jnp.float32), axis=0)
    target_grad = out_cotangent.astype(jnp.float32) + norm_back(
        target_rows, target_gain, d_normed_t
    )
    attended_rows = attended_all.reshape(sp_n, tp_n, target_local, local_width)
    out_weight_grad = jnp.einsum(
        "stlw,tsld->wd", attended_rows, cot_all, preferred_element_type=jnp.float32
    )
    return (target_grad, source_grad, out_weight_grad)


def solution(mesh):
    return jax.shard_map(
        body,
        mesh=mesh,
        in_specs=(
            P(("sp", "tp"), None),
            P(("sp", "tp"), None),
            P(),
            P(),
            P(None, "tp"),
            P("tp", None),
            P("tp", None),
            P("tp", None),
            P(("sp", "tp"), None),
        ),
        out_specs=(P(("sp", "tp"), None), P(("sp", "tp"), None), P("tp", None)),
        check_vma=False,
    )
```

profile of v0, /device:TPU:0, one launch (start us, length us, event | category | flops | bytes accessed | tf_op | source)
XLA Modules:
  0.0 180.8 jit_solution(7068406512579299944)
XLA Ops:
  0.6 0.0 copy-start
  0.6 1.1 fusion.50
  1.8 1.2 fusion.44
  3.0 1.6 fusion.61.refs_0_
  4.6 17.3 %shard_map.112 = (bf16[8,1,24,2048]{3,2,1,0:T(8,128)(2,1)}, bf16[8,1,24,2048]{3,2,1,0:T(8,128)(2,1)}) custom-call(bf16[1,24,2048]{2,1,0:T(8,128)(2,1)} %fusion.61.refs_0_, bf16[1,24,2048]{2,1,0:T(8,128)(2,1)} %bitcast.227), custom_call_target="tpu_custom_call" | custom-call | tf_op jit(solution)/shard_map/pallas_call | solution.py:226
  22.0 0.0 copy-done
  22.0 2.2 %convolution_convert_fusion.4 = bf16[192,256]{1,0:T(8,128)(2,1)} fusion(bf16[192,2048]{1,0:T(8,128)(2,1)} %bitcast.233, bf16[2048,256]{1,0:T(8,128)(2,1)S(1)} %copy-done), kind=kOutput, calls=%fused_computation.42 | convolution fusion | flops 201375744 | bytes 1933312 | tf_op jit(solution)/shard_map/dot_general | solution.py:241
  24.1 2.6 %convolution_convert_fusion.3 = bf16[192,256]{1,0:T(8,128)(2,1)} fusion(bf16[192,2048]{1,0:T(8,128)(2,1)} %bitcast.232, bf16[256,2048]{1,0:T(8,128)(2,1)} %param.16), kind=kOutput, calls=%fused_computation.41 | convolution fusion | flops 201375744 | bytes 1933312 | tf_op jit(solution)/shard_map/dot_general | solution.py:241
  26.8 31.9 %shard_map.113 = (bf16[8,2,128,512]{3,2,1,0:T(8,128)(2,1)}, bf16[8,2,128,512]{3,2,1,0:T(8,128)(2,1)}, bf16[4,2,96,256]{3,2,1,0:T(8,128)(2,1)}, bf16[4,2,96,256]{3,2,1,0:T(8,128)(2,1)}, bf16[4,1,24,2048]{3,2,1,0:T(8,128)(2,1)}) custom-call(bf16[2,128,512]{2,1,0:T(8,128)(2,1)} %bitcast.244, bf16[2,128,512]{2,1,0:T(8,128)(2,1)} %bitcast.245, ...), custom_call_target="tpu_custom_call" | custom-call | tf_op jit(solution)/shard_map/pallas_call | solution.py:226
  58.7 2.3 %convolution_convert_fusion.1 = bf16[128,512]{1,0:T(8,128)(2,1)S(1)} fusion(bf16[2048,512]{1,0:T(8,128)(2,1)} %bitcast.219, bf16[128,2048]{1,0:T(8,128)(2,1)} %param.10, f32[2048]{0:T(1024)} %param.12, f32[128]{0:T(128)S(1)} %get-tuple-element.38), kind=kOutput, calls=%fused_computation.39 | convolution fusion | flops 269549568 | bytes 2761216 | tf_op jit(solution)/shard_map/dot_general | solution.py:241
  61.0 0.1 copy.31
  61.1 0.2 copy.32
  61.3 2.3 %convolution_convert_fusion.2 = bf16[128,512]{1,0:T(8,128)(2,1)S(1)} fusion(bf16[2048,512]{1,0:T(8,128)(2,1)} %bitcast.221, bf16[128,2048]{1,0:T(8,128)(2,1)} %param.10, f32[2048]{0:T(1024)} %param.12, f32[128]{0:T(128)S(1)} %get-tuple-element.38), kind=kOutput, calls=%fused_computation.40 | convolution fusion | flops 269549568 | bytes 2761216 | tf_op jit(solution)/shard_map/dot_general | solution.py:241
  63.6 0.1 copy.29
  63.7 0.2 copy.30
  63.9 0.9 pad_maximum_fusion.refs_0_
  64.7 8.3 %shard_map.114 = bf16[8,128,128]{2,1,0:T(8,128)(2,1)} custom-call(bf16[8,128,128]{2,1,0:T(8,128)(2,1)} %pad_maximum_fusion.refs_0_), custom_call_target="tpu_custom_call" | custom-call | tf_op jit(solution)/shard_map/pallas_call | solution.py:226
  73.1 1.1 copy.33
  74.2 0.1 reshape.290
  74.3 1.3 copy.35
  75.6 0.4 reshape.292
  76.1 1.3 copy.37
  77.4 0.4 reshape.294
  77.8 1.8 %bitcast_reduce_fusion = (f32[4,768]{1,0:T(4,128)S(1)}, f32[1024,768,4]{1,0,2:T(8,128)S(1)}) fusion(bf16[768,4,64]{0,2,1:T(8,128)(2,1)S(1)} %reshape.292, bf16[1024,2,1,64]{0,3,2,1:T(8,128)(2,1)S(1)} %bitcast.215), kind=kOutput, calls=%fused_computation.6 | convolution fusion | flops 408941568 | bytes 13119488 | tf_op jit(solution)/shard_map/tgqd,sgd->gqts/dot_general | solution.py:245
  79.6 0.0 copy-start.1
  79.6 6.9 %fusion.14 = (f32[4,768]{1,0:T(4,128)S(1)}, f32[4,768]{1,0:T(4,128)S(1)}, f32[1024,768,4]{1,0,2:T(8,128)}) fusion(f32[4,768]{1,0:T(4,128)S(1)} %get-tuple-element.41, f32[1024,768,4]{1,0,2:T(8,128)S(1)} %get-tuple-element.42, bf16[768,4,64]{0,2,1:T(8,128)(2,1)S(1)} %reshape.294, bf16[1024,2,1,64]{0,3,2,1:T(8,128)(2,1)S(1)} %bitcast.216), kind=kOutput, calls=%fused_computation.16 | convolution fusion | flops 418375680 | bytes 25726976 | tf_op jit(solution)/shard_map/tgqd,sgd->gqts/dot_general | solution.py:245
  86.5 1.4 copy-done.1
  88.0 0.6 reshape.295.refs_0_
  88.6 9.0 %shard_map.115 = f32[4,12,768]{2,1,0:T(8,128)} custom-call(f32[12,768]{1,0:T(8,128)} %reshape.295.refs_0_), custom_call_target="tpu_custom_call" | custom-call | tf_op jit(solution)/shard_map/pallas_call | solution.py:226
  97.6 0.0 copy-start.2
  97.7 1.2 copy.38
  98.9 0.1 fusion.65
  99.0 6.3 %fusion.40 = bf16[1024,1,64]{0,2,1:T(8,128)(2,1)S(1)} fusion(bf16[768,4,64]{0,2,1:T(8,128)(2,1)S(1)} %reshape.294, f32[4,768]{1,0:T(4,128)S(1)} %get-tuple-element.35, f32[4,768]{1,0:T(4,128)S(1)} %get-tuple-element.41, f32[1024,768,4]{1,0,2:T(8,128)} %copy-done.1), kind=kOutput, calls=%fused_computation.43 | convolution fusion | flops 415301632 | bytes 13131776 | tf_op jit(solution)/shard_map/gqts,tgqd->sgd/dot_general | solution.py:245
  105.3 0.6 copy-done.2
  105.9 6.8 %fusion.7 = bf16[4,768,1024]{1,2,0:T(8,128)(2,1)S(1)} fusion(f32[1024,768,4]{1,0,2:T(8,128)} %get-tuple-element.43, f32[4,768]{1,0:T(4,128)S(1)} %get-tuple-element.36, f32[4,768]{1,0:T(4,128)S(1)} %get-tuple-element.35, f32[4,768]{1,0:T(4,128)S(1)} %get-tuple-element.41, f32[1024,768,4]{1,0,2:T(8,128)S(1)} %copy-done.2), kind=kLoop, calls=%fused_computation.11 | loop fusion | flops 18874368 | bytes 31494144 | tf_op jit(solution)/shard_map/reshape.11
  112.7 2.0 %fusion.43 = bf16[1024,1,64]{0,2,1:T(8,128)(2,1)S(1)} fusion(bf16[768,4,64]{0,2,1:T(8,128)(2,1)S(1)} %reshape.292, bf16[4,768,1024]{1,2,0:T(8,128)(2,1)S(1)} %fusion.7), kind=kOutput, calls=%fused_computation.44 | convolution fusion | flops 402784256 | bytes 6815744 | tf_op jit(solution)/shard_map/gqts,tgqd->sgd/dot_general | solution.py:245
  114.7 1.2 fusion.31
  115.9 0.0 copy-start.3
  115.9 0.0 copy-start.8
  115.9 2.3 %fusion.28 = bf16[768,1,4,64]{0,3,2,1:T(8,128)(2,1)S(1)} fusion(f32[4,768]{1,0:T(4,128)S(1)} %get-tuple-element.41, f32[1024,768,4]{1,0,2:T(8,128)S(1)} %copy-done.2, f32[768,4]{0,1:T(4,128)S(1)} %bitcast.246, bf16[1024,2,1,64]{0,3,2,1:T(8,128)(2,1)S(1)} %bitcast.218), kind=kOutput, calls=%fused_computation.32 | convolution fusion | flops 412483584 | bytes 13131776 | tf_op jit(solution)/shard_map/gqts,sgd->tgqd/dot_general | solution.py:245
  118.2 0.5 convert_element_type.97
  118.7 1.1 copy.48.refs_1_
  119.8 0.5 convert_element_type.94
  120.2 1.1 copy.47.refs_0_
  121.3 0.2 copy.44
  121.5 0.2 copy.46
  121.7 0.0 copy-start.5
  121.7 0.0 copy-start.7
  121.7 0.9 pad_maximum_fusion.1.refs_2_
  122.6 25.4 %shard_map.116 = (bf16[4,192,256]{2,1,0:T(8,128)(2,1)}, bf16[4,192,256]{2,1,0:T(8,128)(2,1)}, bf16[8,128,128]{2,1,0:T(8,128)(2,1)}, bf16[8,4,24,2048]{3,2,1,0:T(8,128)(2,1)}) custom-call(bf16[4,192,256]{2,1,0:T(8,128)(2,1)} %copy.47.refs_0_, bf16[4,192,256]{2,1,0:T(8,128)(2,1)} %copy.48.refs_1_, bf16[8,128,128]{2,1,0:T(8,128)(2,1)} %pad_maximum_fusion.1.refs_2_, ...), custom_call_target="tpu_custom_call" | custom-call | tf_op jit(solution)/shard_map/pallas_call | solution.py:226
  148.0 1.1 reduce_sum.127
  149.0 1.7 reduce_sum.128
  150.7 1.2 slice_bitcast_fusion
  151.9 0.1 copy.50
  152.1 0.1 copy.49
  152.2 2.6 %fusion.69 = f32[128,2048]{1,0:T(8,128)S(1)} fusion(bf16[128,512]{0,1:T(8,128)(2,1)S(1)} %bitcast.235, bf16[2048,512]{1,0:T(8,128)(2,1)} %bitcast.222), kind=kOutput, calls=%fused_computation.90 | convolution fusion | flops 268435456 | bytes 3276800 | tf_op jit(solution)/shard_map/dot_general | solution.py:241
  154.8 2.5 %fusion.49 = (f32[128]{0:T(128)S(1)}, f32[128,2048]{1,0:T(8,128)S(1)}) fusion(bf16[128,2048]{1,0:T(8,128)(2,1)S(1)} %copy-done.3, f32[2048]{0:T(1024)S(1)} %copy-done.8, f32[128,2048]{1,0:T(8,128)S(1)} %fusion.69, bf16[128,512]{0,1:T(8,128)(2,1)S(1)} %bitcast.234, bf16[2048,512]{1,0:T(8,128)(2,1)} %bitcast.220), kind=kOutput, calls=%fused_computation.50 | convolution fusion | flops 269746048 | bytes 4858368 | tf_op jit(solution)/shard_map/dot_general | solution.py:241
  157.3 1.3 fusion.48
  158.7 1.4 convolution_convert_fusion
  160.0 15.2 %shard_map.117 = (bf16[8,24,2048]{2,1,0:T(8,128)(2,1)}, bf16[4,2,96,256]{3,2,1,0:T(8,128)(2,1)}) custom-call(bf16[8,24,2048]{2,1,0:T(8,128)(2,1)} %bitcast.214, bf16[2,96,256]{2,1,0:T(8,128)(2,1)} %bitcast.239), custom_call_target="tpu_custom_call" | custom-call | tf_op jit(solution)/shard_map/pallas_call | solution.py:226
  175.2 1.3 convert_reduce_fusion
  176.5 3.3 %fusion.17 = f32[256,2048]{1,0:T(8,128)} fusion(bf16[4,8,24,256]{3,2,1,0:T(8,128)(2,1)} %bitcast.243, bf16[8,4,24,2048]{3,2,1,0:T(8,128)(2,1)S(1)} %copy-done.4), kind=kOutput, calls=%fused_computation.19 | convolution fusion | flops 805306368 | bytes 5636096 | tf_op jit(solution)/shard_map/stlw,tsld->wd/dot_general | solution.py:373
  179.8 0.1 fusion.56
  180.0 0.8 fusion.55
  (15 shorter events, 0.1 us)
Async XLA Ops:
  0.6 21.3 %copy-start = (bf16[2048,256]{1,0:T(8,128)(2,1)S(1)}, bf16[2048,256]{1,0:T(8,128)(2,1)}, u32[]{:S(2)}) copy-start(bf16[2048,256]{1,0:T(8,128)(2,1)} %param.13) | copy-start | bytes 3145732
  79.6 8.3 %copy-start.1 = (f32[1024,768,4]{1,0,2:T(8,128)}, f32[1024,768,4]{1,0,2:T(8,128)S(1)}, u32[]{:S(2)}) copy-start(f32[1024,768,4]{1,0,2:T(8,128)S(1)} %get-tuple-element.42) | copy-start | bytes 37748740
  97.6 8.3 %copy-start.2 = (f32[1024,768,4]{1,0,2:T(8,128)S(1)}, f32[1024,768,4]{1,0,2:T(8,128)}, u32[]{:S(2)}) copy-start(f32[1024,768,4]{1,0,2:T(8,128)} %copy-done.1) | copy-start | bytes 37748740
  115.9 38.9 %copy-start.3 = (bf16[128,2048]{1,0:T(8,128)(2,1)S(1)}, bf16[128,2048]{1,0:T(8,128)(2,1)}, u32[]{:S(2)}) copy-start(bf16[128,2048]{1,0:T(8,128)(2,1)} %param.10) | copy-start | bytes 1572868
  115.9 38.9 %copy-start.8 = (f32[2048]{0:T(1024)S(1)}, f32[2048]{0:T(1024)}, u32[]{:S(2)}) copy-start(f32[2048]{0:T(1024)} %param.12) | copy-start | bytes 24580
  121.7 58.2 %copy-start.5 = (bf16[24,2048]{1,0:T(8,128)(2,1)S(1)}, bf16[24,2048]{1,0:T(8,128)(2,1)}, u32[]{:S(2)}) copy-start(bf16[24,2048]{1,0:T(8,128)(2,1)} %param.9) | copy-start | bytes 294916
  121.7 58.1 %copy-start.7 = (f32[2048]{0:T(1024)S(1)}, f32[2048]{0:T(1024)}, u32[]{:S(2)}) copy-start(f32[2048]{0:T(1024)} %param.11) | copy-start | bytes 24580
  122.6 57.4 %copy-start.6 = (bf16[24,2048]{1,0:T(8,128)(2,1)S(1)}, bf16[24,2048]{1,0:T(8,128)(2,1)}, u32[]{:S(2)}) copy-start(bf16[24,2048]{1,0:T(8,128)(2,1)} %param.17) | copy-start | bytes 294916
  152.2 24.3 %copy-start.4 = (bf16[8,4,24,2048]{3,2,1,0:T(8,128)(2,1)S(1)}, bf16[8,4,24,2048]{3,2,1,0:T(8,128)(2,1)}, u32[]{:S(2)}) copy-start(bf16[8,4,24,2048]{3,2,1,0:T(8,128)(2,1)} %get-tuple-element.28) | copy-start | bytes 9437188
where the time goes:
time: 182 us; the launch traced here: 181 us
  Pallas kernels  107 us (59%)
  matrix products  39.7 us (22%)
  other arithmetic  19 us (10%)
  local copies, waits for them, and re-layouts  14 us (8%)
    pallas_call x6, Pallas kernels, exchange(): pl.pallas_call(functools.partial(exchange_kernel, kinds, sp_n, tp_n), out...  107 us
    dot_general x6, matrix products, einsum(): return jnp.einsum(text, left, right, preferred_element_type=jnp.float32)  20.6 us
    dot_general x7, matrix products, matmul(): return jnp.dot(left, right, preferred_element_type=jnp.float32)  15.8 us
    another operation x1, other arithmetic  6.77 us
    pallas_call x4, local copies, waits for them, and re-layouts, exchange(): pl.pallas_call(functools.partial(exchange_kernel, kinds, sp_n, tp_n), out...  4.91 us

commit v1 on v0

--- a/solution.py
+++ b/solution.py
@@ -376,9 +376,481 @@
     return (target_grad, source_grad, out_weight_grad)
 
 
+def fused_kernel(sp_n, tp_n, *refs):
+    target, source, tgain, sgain, qw, kw, vw, ow, cot = refs[:9]
+    tgrad, sgrad, owg = refs[9:12]
+    (t_rx, c_rx, rows, cotf, w_rx, ns, q_all, d_all, kv_tx, kv_rx, k2, v2, kvt) = refs[12:25]
+    (qc, dc, p_buf, dp_buf, st, o_tx, o_rx, att, attb, dq_tx, dq_rx, qg) = refs[25:37]
+    (dk, dv, g_tx, g_rx, gcat, tt, tp_rx, ts_tx, ts_rx, un, share) = refs[37:48]
+    send_s, t_s, c_s, w_s, cz_s, q_s, d_s, kv_s = refs[48:56]
+    st_s, o_s, att_s, dq_s, g_s, tp_s, ts_s = refs[56:63]
+    f32, bf16 = jnp.float32, jnp.bfloat16
+    z, me = lax.axis_index("sp"), lax.axis_index("tp")
+    core = lax.rem(me, 2)
+    t_loc, width = target.shape
+    s_loc = source.shape[0]
+    slab, local_width = w_rx.shape[2], qw.shape[1]
+    heads = local_width // HEAD_DIM
+    t_block = tp_n * t_loc
+    lanes = heads * t_block
+    s_block = tp_n * s_loc
+    pairs = w_rx.shape[0]
+    scale = HEAD_DIM ** (-0.5)
+
+    def across(i):
+        return i + 2 - 4 * lax.rem(i // 2, 2)
+
+    def along(i):
+        return i + 4 - 8 * lax.rem(i // 4, 2)
+
+    mate = me + 1 - 2 * core
+    zs = [lax.rem(z + k, sp_n) for k in range(1, sp_n)]
+    ts = [lax.rem(me + k, tp_n) for k in range(1, tp_n)]
+
+    barrier = pltpu.get_barrier_semaphore()
+    for peer in zs:
+        pl.semaphore_signal(barrier, inc=1, device_id=(peer, me), device_id_type=MESH)
+    for peer in ts:
+        pl.semaphore_signal(barrier, inc=1, device_id=(z, peer), device_id_type=MESH)
+
+    sent = []
+
+    def push(src, dst, sem, zz, i, when=None):
+        one = pltpu.make_async_remote_copy(
+            src_ref=src,
+            dst_ref=dst,
+            send_sem=send_s.at[len(sent)],
+            recv_sem=sem,
+            device_id=(zz, i),
+            device_id_type=MESH,
+        )
+        sent.append((one, when))
+        if when is None:
+            one.start()
+        else:
+            pl.when(when)(lambda: one.start())
+
+    def pull(ref, sem):
+        pltpu.make_async_remote_copy(
+            src_ref=ref,
+            dst_ref=ref,
+            send_sem=send_s.at[0],
+            recv_sem=sem,
+            device_id=(z, mate),
+            device_id_type=MESH,
+        ).wait_recv()
+
+    def nt(a, b):
+        return lax.dot_general(a, b, (((1,), (1,)), ((), ())), preferred_element_type=f32)
+
+    def nn(a, b):
+        return jnp.dot(a, b, preferred_element_type=f32)
+
+    class Gather:
+        def __init__(self, slot, sem, turn):
+            self.slot, self.sem, self.turn = slot, sem, turn
+
+        def start(self):
+            for peer in (across(me), along(me), mate):
+                push(self.slot(me), self.slot(me), self.sem(me), z, peer)
+
+        def mid(self):
+            for order, origin in enumerate((across(me), along(me))):
+                piece, sem = self.slot(origin), self.sem(origin)
+                pull(piece, sem)
+                if order == self.turn:
+                    push(piece, piece, sem, z, along(me) if order == 0 else across(me))
+                push(piece, piece, sem, z, mate)
+
+        def fin(self):
+            origin = across(along(me))
+            piece, sem = self.slot(origin), self.sem(origin)
+            pull(piece, sem)
+            push(piece, piece, sem, z, mate)
+
+        def rest(self):
+            for origin in (mate, across(mate), along(mate), across(along(mate))):
+                pull(self.slot(origin), self.sem(origin))
+
+    t_rx[me] = normalize(target[...], tgain[...])
+    c_rx[z, me] = cot[...]
+    pl.semaphore_wait(barrier, sp_n - 1 + tp_n - 1)
+
+    t_all = Gather(lambda o: t_rx.at[o], lambda o: t_s.at[o], 0)
+    c_own = Gather(lambda o: c_rx.at[z, o], lambda o: c_s.at[z * tp_n + o], 1)
+    w_all = [
+        Gather(lambda o, c=c: w_rx.at[c, o], lambda o, c=c: w_s.at[c * tp_n + o], c % 2)
+        for c in range(pairs)
+    ]
+    c_far = [
+        Gather(lambda o, p=p: c_rx.at[p, o], lambda o, p=p: c_s.at[p * tp_n + o], k % 2)
+        for k, p in enumerate(zs)
+    ]
+
+    t_all.start()
+    c_own.start()
+    for peer in zs:
+        push(c_rx.at[z, me], c_rx.at[z, me], cz_s.at[z], peer, me)
+    for c in range(pairs):
+        for j in range(2):
+            head = 2 * c + j
+            cols = slice(head * HEAD_DIM, (head + 1) * HEAD_DIM)
+            both = jnp.concatenate([kw[:, cols], vw[:, cols]], axis=1)
+            w_rx[c, me, :, j * 2 * HEAD_DIM : (j + 1) * 2 * HEAD_DIM] = both
+    t_all.mid()
+    c_own.mid()
+    for c in range(pairs):
+        w_all[c].start()
+    step = min(s_loc, 32)
+    for i in range(0, s_loc, step):
+        ns[i : i + step] = normalize(source[i : i + step], sgain[...])
+    t_all.fin()
+    c_own.fin()
+    t_all.rest()
+    for o in range(tp_n):
+        rows[o * t_loc : (o + 1) * t_loc] = t_rx[o]
+    q_all[z] = (nn(rows[...], qw[...]).astype(bf16) * scale).astype(bf16)
+    for peer in zs:
+        push(q_all.at[z], q_all.at[z], q_s.at[z], peer, me)
+    c_own.rest()
+    for o in range(tp_n):
+        cotf[z, o * t_loc : (o + 1) * t_loc] = c_rx[z, o]
+    d_all[z] = nt(cotf[z], ow[...]).astype(bf16)
+    for peer in zs:
+        push(d_all.at[z], d_all.at[z], d_s.at[z], peer, me)
+
+    def split_kv(c):
+        w_all[c].rest()
+        total = nn(ns[:, :slab], w_rx[c, 0])
+        for o in range(1, tp_n):
+            total += nn(ns[:, o * slab : (o + 1) * slab], w_rx[c, o])
+        total = total.astype(bf16)
+        for j in range(2):
+            head = 2 * c + j
+            part = total[:, j * 2 * HEAD_DIM : (j + 1) * 2 * HEAD_DIM]
+            kv_tx[head] = part
+
+            @pl.when(me == head)
+            def _():
+                kv_rx[head] = part
+
+            push(kv_tx.at[head], kv_rx.at[me], kv_s.at[me], z, head, me != head)
+
+    for c in range(pairs):
+        w_all[c].mid()
+        if c >= 1:
+            w_all[c - 1].fin()
+        if c >= 2:
+            split_kv(c - 2)
+    split_kv(pairs - 2)
+    w_all[pairs - 1].fin()
+    split_kv(pairs - 1)
+    for k, p in enumerate(zs):
+        pull(c_rx.at[p, me], cz_s.at[p])
+        c_far[k].start()
+    for p in zs:
+        pull(q_all.at[p], q_s.at[p])
+        pull(d_all.at[p], d_s.at[p])
+    for b in range(sp_n):
+        for h in range(heads):
+            cols = slice(h * HEAD_DIM, (h + 1) * HEAD_DIM)
+            qc[b, h * t_block : (h + 1) * t_block] = q_all[b, :, cols]
+            dc[b, h * t_block : (h + 1) * t_block] = d_all[b, :, cols]
+    for o in ts:
+        pull(kv_rx.at[o], kv_s.at[o])
+    for o in range(tp_n):
+        part = kv_rx[o]
+        k2[o * s_loc : (o + 1) * s_loc] = part[:, :HEAD_DIM]
+        v2[o * s_loc : (o + 1) * s_loc] = part[:, HEAD_DIM:]
+        kvt[:, o * s_loc : (o + 1) * s_loc] = part.astype(f32).T.astype(bf16)
+
+    tile = 256
+    steps = lanes // tile
+
+    def first(b):
+        def body(j, carry):
+            cols = pl.ds(pl.multiple_of(j * tile, tile), tile)
+            score = nt(k2[...], qc[b, cols])
+            top = jnp.max(score, axis=0, keepdims=True)
+            weight = jnp.exp(score - top)
+            d_prob = nt(v2[...], dc[b, cols])
+            total = jnp.sum(weight, axis=0, keepdims=True)
+            inner = jnp.sum(weight * d_prob, axis=0, keepdims=True)
+            p_buf[b, :, cols] = weight
+            dp_buf[b, :, cols] = d_prob
+            o_tx[b, :, cols] = nn(kvt[HEAD_DIM:], weight.astype(bf16)).astype(bf16)
+            filler = jnp.zeros((5, tile), f32)
+            st[b, z, :, cols] = jnp.concatenate([top, total, inner, filler], axis=0)
+            return carry
+
+        lax.fori_loop(0, steps, body, 0)
+        for peer in zs:
+            push(st.at[b, z], st.at[b, z], st_s.at[b * sp_n + z], peer, me)
+        push(o_tx.at[b], o_rx.at[z], o_s.at[z], b, me, z != b)
+
+    for b in range(sp_n):
+        first(b)
+        if b < len(c_far):
+            c_far[b].mid()
+        if b >= 1 and b - 1 < len(c_far):
+            c_far[b - 1].fin()
+    for k in range(sp_n - 1, len(c_far)):
+        c_far[k].fin()
+
+    def stats(b):
+        tops = [st[b, s, 0:1] for s in range(sp_n)]
+        row_max = functools.reduce(jnp.maximum, tops)
+        lifts = [jnp.exp(top - row_max) for top in tops]
+        total = sum(st[b, s, 1:2] * lifts[s] for s in range(sp_n))
+        inner = sum(st[b, s, 2:3] * lifts[s] for s in range(sp_n))
+        return row_max, lifts, total, inner / total
+
+    def stats_in(b):
+        for p in zs:
+            pull(st.at[b, p], st_s.at[b * sp_n + p])
+
+    def attend():
+        for p in zs:
+            pull(o_rx.at[p], o_s.at[p])
+        row_max, lifts, total, inner = stats(z)
+        o_rx[z] = o_tx[z]
+        mixed = sum(o_rx[s].astype(f32) * lifts[s] for s in range(sp_n))
+        att[z] = (mixed / total).astype(bf16)
+        for peer in zs:
+            push(att.at[z], att.at[z], att_s.at[z], peer, me)
+
+    def second(i):
+        b = z if i == sp_n - 1 else i + (i >= z).astype(jnp.int32)
+        if i < sp_n - 1:
+            stats_in(b)
+        row_max, lifts, total, inner = stats(b)
+        share[0:1] = jnp.exp(st[b, z, 0:1] - row_max) / total
+        share[1:2] = inner
+
+        def body(j, carry):
+            cols = pl.ds(pl.multiple_of(j * tile, tile), tile)
+            prob = p_buf[b, :, cols] * share[0:1, cols]
+            d_score = (prob * (dp_buf[b, :, cols] - share[1:2, cols])).astype(bf16)
+            prob = prob.astype(bf16)
+            dv[...] += nn(prob, dc[b, cols])
+            dk[...] += nn(d_score, qc[b, cols])
+            dq_tx[b, :, cols] = nn(kvt[:HEAD_DIM], d_score).astype(bf16)
+            return carry
+
+        lax.fori_loop(0, steps, body, 0)
+        if i < sp_n - 1:
+            push(dq_tx.at[b], dq_rx.at[z], dq_s.at[z], b, me)
+
+    dk[...] = jnp.zeros_like(dk)
+    dv[...] = jnp.zeros_like(dv)
+    for i in range(sp_n):
+        second(i)
+        if i == 0:
+            stats_in(z)
+            attend()
+
+    for o in range(tp_n):
+        part = slice(o * s_loc, (o + 1) * s_loc)
+        g_tx[o] = jnp.concatenate([dk[part], dv[part]], axis=1).astype(bf16)
+    for o in ts:
+        push(g_tx.at[o], g_rx.at[me], g_s.at[me], z, o)
+    g_rx[me] = g_tx[me]
+
+    for p in zs:
+        pull(dq_rx.at[p], dq_s.at[p])
+    dq_rx[z] = dq_tx[z]
+    summed = sum(dq_rx[s].astype(f32) for s in range(sp_n)) * scale
+    summed = summed.T
+    for h in range(heads):
+        piece = summed[h * t_block : (h + 1) * t_block].astype(bf16)
+        qg[:, h * HEAD_DIM : (h + 1) * HEAD_DIM] = piece
+
+    wide = 512
+
+    def terms(j, carry):
+        cols = pl.ds(pl.multiple_of(j * wide, wide), wide)
+        value = nt(qg[...], qw[cols])
+        for o in range(tp_n):
+            tt[o, :, cols] = value[o * t_loc : (o + 1) * t_loc].astype(bf16)
+        return carry
+
+    lax.fori_loop(0, width // wide, terms, 0)
+    chips = tp_n // 2
+    for c in range(chips):
+        push(tt.at[2 * c + 1 - core], tp_rx.at[c], tp_s.at[c], z, mate)
+    for c in range(chips):
+        pull(tp_rx.at[c], tp_s.at[c])
+        ts_tx[c] = (tt[2 * c + core].astype(f32) + tp_rx[c].astype(f32)).astype(bf16)
+    for r, peer in enumerate((across(along(me)), across(me), along(me))):
+        push(ts_tx.at[peer // 2], ts_rx.at[r], ts_s.at[r], z, peer)
+
+    for k, p in enumerate(zs):
+        c_far[k].rest()
+        for o in range(tp_n):
+            cotf[p, o * t_loc : (o + 1) * t_loc] = c_rx[p, o]
+    for p in zs:
+        pull(att.at[p], att_s.at[p])
+    for b in range(sp_n):
+        for h in range(heads):
+            piece = att[b, :, h * t_block : (h + 1) * t_block]
+            attb[b, h * HEAD_DIM : (h + 1) * HEAD_DIM] = piece
+
+    def weight_grad(j, carry):
+        cols = pl.ds(pl.multiple_of(j * tile, tile), tile)
+        total = nn(attb[0], cotf[0, :, cols])
+        for b in range(1, sp_n):
+            total += nn(attb[b], cotf[b, :, cols])
+        owg[:, cols] = total
+        return carry
+
+    lax.fori_loop(0, width // tile, weight_grad, 0)
+
+    for o in ts:
+        pull(g_rx.at[o], g_s.at[o])
+    for o in range(tp_n):
+        gcat[:, o * 2 * HEAD_DIM : (o + 1) * 2 * HEAD_DIM] = g_rx[o]
+
+    def upstream(o, carry):
+        cols = pl.ds(pl.multiple_of(o * slab, slab), slab)
+        total = nt(gcat[:, : 4 * HEAD_DIM], w_rx[0, o])
+        for c in range(1, pairs):
+            total += nt(gcat[:, c * 4 * HEAD_DIM : (c + 1) * 4 * HEAD_DIM], w_rx[c, o])
+        un[:, cols] = total
+        return carry
+
+    lax.fori_loop(0, tp_n, upstream, 0)
+    for i in range(0, s_loc, step):
+        part = slice(i, i + step)
+        sgrad[part] = norm_back(source[part], sgain[...], un[part])
+
+    mine = ts_tx[me // 2].astype(f32)
+    for r in range(3):
+        pull(ts_rx.at[r], ts_s.at[r])
+    mine = mine + sum(ts_rx[r].astype(f32) for r in range(3))
+    tgrad[...] = cot[...].astype(f32) + norm_back(target[...], tgain[...], mine)
+
+    for one, when in sent:
+        if when is None:
+            one.wait_send()
+        else:
+            pl.when(when)(lambda one=one: one.wait_send())
+
+
+def fused_body(
+    target_rows,
+    source_rows,
+    target_gain,
+    source_gain,
+    query_weight,
+    key_weight,
+    value_weight,
+    out_weight,
+    out_cotangent,
+):
+    sp_n, tp_n = lax.axis_size("sp"), lax.axis_size("tp")
+    t_loc, width = target_rows.shape
+    s_loc = source_rows.shape[0]
+    local_width = query_weight.shape[1]
+    heads = local_width // HEAD_DIM
+    t_block, s_block = tp_n * t_loc, tp_n * s_loc
+    lanes = heads * t_block
+    slab = key_weight.shape[0]
+    pairs = KV_HEADS // 2
+    two = 2 * HEAD_DIM
+    f32, bf16 = jnp.float32, jnp.bfloat16
+    vmem, sem = pltpu.VMEM, pltpu.SemaphoreType.DMA
+    scratch = [
+        vmem((tp_n, t_loc, width), bf16),
+        vmem((sp_n, tp_n, t_loc, width), bf16),
+        vmem((t_block, width), bf16),
+        vmem((sp_n, t_block, width), bf16),
+        vmem((pairs, tp_n, slab, 2 * two), bf16),
+        vmem((s_loc, width), bf16),
+        vmem((sp_n, t_block, local_width), bf16),
+        vmem((sp_n, t_block, local_width), bf16),
+        vmem((tp_n, s_loc, two), bf16),
+        vmem((tp_n, s_loc, two), bf16),
+        vmem((s_block, HEAD_DIM), bf16),
+        vmem((s_block, HEAD_DIM), bf16),
+        vmem((two, s_block), bf16),
+        vmem((sp_n, lanes, HEAD_DIM), bf16),
+        vmem((sp_n, lanes, HEAD_DIM), bf16),
+        vmem((sp_n, s_block, lanes), f32),
+        vmem((sp_n, s_block, lanes), f32),
+        vmem((sp_n, sp_n, 8, lanes), f32),
+        vmem((sp_n, HEAD_DIM, lanes), bf16),
+        vmem((sp_n, HEAD_DIM, lanes), bf16),
+        vmem((sp_n, HEAD_DIM, lanes), bf16),
+        vmem((sp_n, local_width, t_block), bf16),
+        vmem((sp_n, HEAD_DIM, lanes), bf16),
+        vmem((sp_n, HEAD_DIM, lanes), bf16),
+        vmem((t_block, local_width), bf16),
+        vmem((s_block, HEAD_DIM), f32),
+        vmem((s_block, HEAD_DIM), f32),
+        vmem((tp_n, s_loc, two), bf16),
+        vmem((tp_n, s_loc, two), bf16),
+        vmem((s_loc, tp_n * two), bf16),
+        vmem((tp_n, t_loc, width), bf16),
+        vmem((tp_n // 2, t_loc, width), bf16),
+        vmem((tp_n // 2, t_loc, width), bf16),
+        vmem((3, t_loc, width), bf16),
+        vmem((s_loc, width), f32),
+        vmem((8, lanes), f32),
+        sem((256,)),
+        sem((tp_n,)),
+        sem((sp_n * tp_n,)),
+        sem((pairs * tp_n,)),
+        sem((sp_n,)),
+        sem((sp_n,)),
+        sem((sp_n,)),
+        sem((tp_n,)),
+        sem((sp_n * sp_n,)),
+        sem((sp_n,)),
+        sem((sp_n,)),
+        sem((sp_n,)),
+        sem((tp_n,)),
+        sem((tp_n // 2,)),
+        sem((3,)),
+    ]
+    return pl.pallas_call(
+        functools.partial(fused_kernel, sp_n, tp_n),
+        out_shape=[
+            jax.ShapeDtypeStruct((t_loc, width), f32),
+            jax.ShapeDtypeStruct((s_loc, width), f32),
+            jax.ShapeDtypeStruct((local_width, width), f32),
+        ],
+        in_specs=[pl.BlockSpec(memory_space=pltpu.VMEM)] * 9,
+        out_specs=[pl.BlockSpec(memory_space=pltpu.VMEM)] * 3,
+        scratch_shapes=scratch,
+        compiler_params=pltpu.CompilerParams(
+            collective_id=0,
+            has_side_effects=True,
+            vmem_limit_bytes=67043328,
+        ),
+    )(
+        target_rows,
+        source_rows,
+        target_gain[None],
+        source_gain[None],
+        query_weight,
+        key_weight,
+        value_weight,
+        out_weight,
+        out_cotangent,
+    )
+
+
+def choose(*args):
+    square = lax.axis_size("tp") == 8 and KV_HEADS == 8
+    lanes = lax.axis_size("tp") * args[0].shape[0] * args[4].shape[1] // HEAD_DIM
+    if square and lanes % 256 == 0:
+        return fused_body(*args)
+    return body(*args)
+
+
 def solution(mesh):
     return jax.shard_map(
-        body,
+        choose,
         mesh=mesh,
         in_specs=(
             P(("sp", "tp"), None),

time: 182 us -> 102 us (0.56)
  the two profiles are of different devices: /device:TPU:0 before, /device:TPU:19 now
where the time goes in v1:
time: 102 us
  Pallas kernels  95.7 us (94%)
  local copies, waits for them, and re-layouts  5.38 us (5%)
    pallas_call x1, Pallas kernels, fused_body(): pl.pallas_call(functools.partial(fused_kernel, sp_n, tp_n), out_shape=[ja...  95.7 us
    unnamed x5, local copies, waits for them, and re-layouts  5.38 us

profile of v1, /device:TPU:19, one launch (start us, length us, event | category | flops | bytes accessed | tf_op | source)
XLA Modules:
  0.0 101.7 jit_solution(15878723100779142720)
XLA Ops:
  0.6 95.7 %shard_map.112 = (f32[24,2048]{1,0:T(8,128)}, f32[128,2048]{1,0:T(8,128)}, f32[256,2048]{1,0:T(8,128)}) custom-call(bf16[24,2048]{1,0:T(8,128)(2,1)} %refs_0_.1, bf16[128,2048]{1,0:T(8,128)(2,1)} %refs_1_.1, f32[1,2048]{1,0:T(1,128)} %bitcast.2, f32[1,2048]{1,0:T(1,128)} %bitcast.3, bf16[2048,256]{1,0:T(8,128)(2,1)} %refs_4_.1, bf16[256,512]{1,0:T(8,128)(2,1)} %refs_5_.1, ...), custom_call_target="tpu_custom_call" | custom-call | tf_op jit(solution)/shard_map/pallas_call | solution.py:815
  96.3 0.0 copy-start
  96.3 1.8 %copy.15 = f32[24,2048]{1,0:T(8,128)} copy(f32[24,2048]{1,0:T(8,128)} %get-tuple-element.6) | data formatting | bytes 393216
  98.1 2.3 %copy.16 = f32[128,2048]{1,0:T(8,128)} copy(f32[128,2048]{1,0:T(8,128)} %get-tuple-element.7) | data formatting | bytes 2097152
  100.4 0.0 copy-done
  100.4 1.3 %copy.17 = f32[256,2048]{1,0:T(8,128)} copy(f32[256,2048]{1,0:T(8,128)S(1)} %copy-done) | data formatting | bytes 4194304
Async XLA Ops:
  96.3 4.1 %copy-start = (f32[256,2048]{1,0:T(8,128)S(1)}, f32[256,2048]{1,0:T(8,128)}, u32[]{:S(2)}) copy-start(f32[256,2048]{1,0:T(8,128)} %get-tuple-element.8) | copy-start | bytes 6291460

commit v2 on v1

--- a/solution.py
+++ b/solution.py
@@ -377,13 +377,14 @@
 
 
 def fused_kernel(sp_n, tp_n, *refs):
-    target, source, tgain, sgain, qw, kw, vw, ow, cot = refs[:9]
-    tgrad, sgrad, owg = refs[9:12]
-    (t_rx, c_rx, rows, cotf, w_rx, ns, q_all, d_all, kv_tx, kv_rx, k2, v2, kvt) = refs[12:25]
-    (qc, dc, p_buf, dp_buf, st, o_tx, o_rx, att, attb, dq_tx, dq_rx, qg) = refs[25:37]
-    (dk, dv, g_tx, g_rx, gcat, tt, tp_rx, ts_tx, ts_rx, un, share) = refs[37:48]
-    send_s, t_s, c_s, w_s, cz_s, q_s, d_s, kv_s = refs[48:56]
-    st_s, o_s, att_s, dq_s, g_s, tp_s, ts_s = refs[56:63]
+    loads, stores = refs[:9], refs[9:12]
+    target, source, tgain, sgain, qw, kw, vw, ow = refs[12:20]
+    tgrad, sgrad, owg = refs[20:23]
+    (t_rx, c_rx, rows, cotf, w_rx, ns, q_all, d_all, kv_tx, kv_rx, k2, v2, kvt) = refs[23:36]
+    (qc, dc, p_buf, dp_buf, st, o_tx, o_rx, att, attb, dq_tx, dq_rx, qg) = refs[36:48]
+    (dk, dv, g_tx, g_rx, gcat, tt, tp_rx, ts_tx, ts_rx, un) = refs[48:58]
+    send_s, t_s, c_s, w_s, far_s, cz_s, q_s, d_s, kv_s = refs[58:67]
+    st_s, o_s, att_s, dq_s, g_s, tp_s, ts_s, load_s, store_s = refs[67:76]
     f32, bf16 = jnp.float32, jnp.bfloat16
     z, me = lax.axis_index("sp"), lax.axis_index("tp")
     core = lax.rem(me, 2)
@@ -440,6 +441,16 @@
             device_id_type=MESH,
         ).wait_recv()
 
+    kept = (target, source, tgain, sgain, qw, kw, vw, ow, c_rx.at[z, me])
+    copies = [pltpu.make_async_copy(a, b, load_s.at[i]) for i, (a, b) in enumerate(zip(loads, kept))]
+    for i in (0, 2, 8, 5, 6, 1, 3, 4, 7):
+        copies[i].start()
+
+    def store(i, a):
+        one = pltpu.make_async_copy(a, stores[i], store_s.at[i])
+        one.start()
+        return one
+
     def nt(a, b):
         return lax.dot_general(a, b, (((1,), (1,)), ((), ())), preferred_element_type=f32)
 
@@ -447,74 +458,104 @@
         return jnp.dot(a, b, preferred_element_type=f32)
 
     class Gather:
-        def __init__(self, slot, sem, turn):
-            self.slot, self.sem, self.turn = slot, sem, turn
+        def __init__(self, slot, sem, far, depth):
+            self.slot, self.sem, self.far, self.depth = slot, sem, far, depth
 
         def start(self):
             for peer in (across(me), along(me), mate):
                 push(self.slot(me), self.slot(me), self.sem(me), z, peer)
 
+        def half(self, origin, order):
+            return self.slot(origin).at[self.depth[order] : self.depth[order + 1]]
+
         def mid(self):
             for order, origin in enumerate((across(me), along(me))):
-                piece, sem = self.slot(origin), self.sem(origin)
-                pull(piece, sem)
-                if order == self.turn:
-                    push(piece, piece, sem, z, along(me) if order == 0 else across(me))
-                push(piece, piece, sem, z, mate)
+                pull(self.slot(origin), self.sem(origin))
+                piece = self.half(origin, order)
+                push(piece, piece, self.far(order), z, along(me) if order == 0 else across(me))
+            for origin in (across(me), along(me)):
+                push(self.slot(origin), self.slot(origin), self.sem(origin), z, mate)
 
         def fin(self):
             origin = across(along(me))
-            piece, sem = self.slot(origin), self.sem(origin)
-            pull(piece, sem)
-            push(piece, piece, sem, z, mate)
+            for order in range(2):
+                pull(self.half(origin, order), self.far(order))
+            push(self.slot(origin), self.slot(origin), self.sem(origin), z, mate)
 
         def rest(self):
             for origin in (mate, across(mate), along(mate), across(along(mate))):
                 pull(self.slot(origin), self.sem(origin))
 
+    copies[0].wait()
+    copies[2].wait()
     t_rx[me] = normalize(target[...], tgain[...])
-    c_rx[z, me] = cot[...]
+    copies[8].wait()
     pl.semaphore_wait(barrier, sp_n - 1 + tp_n - 1)
 
-    t_all = Gather(lambda o: t_rx.at[o], lambda o: t_s.at[o], 0)
-    c_own = Gather(lambda o: c_rx.at[z, o], lambda o: c_s.at[z * tp_n + o], 1)
+    some, more = (0, t_loc // 2 // 8 * 8, t_loc), (0, slab // 2, slab)
+    t_all = Gather(lambda o: t_rx.at[o], lambda o: t_s.at[o], lambda k: far_s.at[k], some)
+    c_all = [
+        Gather(
+            lambda o, p=p: c_rx.at[p, o],
+            lambda o, p=p: c_s.at[p * tp_n + o],
+            lambda k, n=n: far_s.at[2 * n + 2 + k],
+            some,
+        )
+        for n, p in enumerate([z] + zs)
+    ]
+    c_own, c_far = c_all[0], c_all[1:]
     w_all = [
-        Gather(lambda o, c=c: w_rx.at[c, o], lambda o, c=c: w_s.at[c * tp_n + o], c % 2)
+        Gather(
+            lambda o, c=c: w_rx.at[c, o],
+            lambda o, c=c: w_s.at[c * tp_n + o],
+            lambda k, c=c: far_s.at[2 * (sp_n + 1 + c) + k],
+            more,
+        )
         for c in range(pairs)
-    ]
-    c_far = [
-        Gather(lambda o, p=p: c_rx.at[p, o], lambda o, p=p: c_s.at[p * tp_n + o], k % 2)
-        for k, p in enumerate(zs)
     ]
 
     t_all.start()
     c_own.start()
     for peer in zs:
         push(c_rx.at[z, me], c_rx.at[z, me], cz_s.at[z], peer, me)
-    for c in range(pairs):
+    copies[5].wait()
+    copies[6].wait()
+
+    def weave(c):
         for j in range(2):
             head = 2 * c + j
             cols = slice(head * HEAD_DIM, (head + 1) * HEAD_DIM)
             both = jnp.concatenate([kw[:, cols], vw[:, cols]], axis=1)
             w_rx[c, me, :, j * 2 * HEAD_DIM : (j + 1) * 2 * HEAD_DIM] = both
-    t_all.mid()
-    c_own.mid()
+
     for c in range(pairs):
-        w_all[c].start()
+        weave(c)
+    w_all[0].start()
+    copies[1].wait()
+    copies[3].wait()
     step = min(s_loc, 32)
     for i in range(0, s_loc, step):
         ns[i : i + step] = normalize(source[i : i + step], sgain[...])
+    t_all.mid()
+    c_own.mid()
+    w_all[1].start()
+    w_all[0].mid()
+    w_all[2].start()
     t_all.fin()
     c_own.fin()
     t_all.rest()
     for o in range(tp_n):
         rows[o * t_loc : (o + 1) * t_loc] = t_rx[o]
+    copies[4].wait()
     q_all[z] = (nn(rows[...], qw[...]).astype(bf16) * scale).astype(bf16)
     for peer in zs:
         push(q_all.at[z], q_all.at[z], q_s.at[z], peer, me)
+    w_all[1].mid()
+    w_all[3].start()
     c_own.rest()
     for o in range(tp_n):
         cotf[z, o * t_loc : (o + 1) * t_loc] = c_rx[z, o]
+    copies[7].wait()
     d_all[z] = nt(cotf[z], ow[...]).astype(bf16)
     for peer in zs:
         push(d_all.at[z], d_all.at[z], d_s.at[z], peer, me)
@@ -536,13 +577,12 @@
 
             push(kv_tx.at[head], kv_rx.at[me], kv_s.at[me], z, head, me != head)
 
-    for c in range(pairs):
+    w_all[0].fin()
+    split_kv(0)
+    for c in range(2, pairs):
         w_all[c].mid()
-        if c >= 1:
-            w_all[c - 1].fin()
-        if c >= 2:
-            split_kv(c - 2)
-    split_kv(pairs - 2)
+        w_all[c - 1].fin()
+        split_kv(c - 1)
     w_all[pairs - 1].fin()
     split_kv(pairs - 1)
     for k, p in enumerate(zs):
@@ -564,30 +604,40 @@
         v2[o * s_loc : (o + 1) * s_loc] = part[:, HEAD_DIM:]
         kvt[:, o * s_loc : (o + 1) * s_loc] = part.astype(f32).T.astype(bf16)
 
-    tile = 256
-    steps = lanes // tile
+    groups = lanes // 128
+
+    def fold(op, x, n=4):
+        size = x.shape[0] // n
+        parts = [
+            op(x[i * size : (i + 1) * size].reshape(size // 8, 8, x.shape[1]), axis=0)
+            for i in range(n)
+        ]
+        both = jnp.maximum if op is jnp.max else jnp.add
+        return op(functools.reduce(both, parts), axis=0, keepdims=True)
+
+    def line(x):
+        return jnp.concatenate([x[g : g + 1] for g in range(groups)], axis=1)
 
     def first(b):
-        def body(j, carry):
-            cols = pl.ds(pl.multiple_of(j * tile, tile), tile)
-            score = nt(k2[...], qc[b, cols])
-            top = jnp.max(score, axis=0, keepdims=True)
-            weight = jnp.exp(score - top)
-            d_prob = nt(v2[...], dc[b, cols])
-            total = jnp.sum(weight, axis=0, keepdims=True)
-            inner = jnp.sum(weight * d_prob, axis=0, keepdims=True)
-            p_buf[b, :, cols] = weight
-            dp_buf[b, :, cols] = d_prob
-            o_tx[b, :, cols] = nn(kvt[HEAD_DIM:], weight.astype(bf16)).astype(bf16)
-            filler = jnp.zeros((5, tile), f32)
-            st[b, z, :, cols] = jnp.concatenate([top, total, inner, filler], axis=0)
-            return carry
-
-        lax.fori_loop(0, steps, body, 0)
+        score = nt(k2[...], qc[b])
+        top = fold(jnp.max, score)
+        weight = jnp.exp(score - top)
+        d_prob = nt(v2[...], dc[b])
+        total = fold(jnp.sum, weight)
+        inner = fold(jnp.sum, weight * d_prob)
+        p_buf[b] = weight
+        dp_buf[b] = d_prob
+        o_tx[b] = nn(kvt[HEAD_DIM:], weight.astype(bf16)).astype(bf16)
+        for k, value in enumerate((top, total, inner)):
+            for g in range(groups):
+                row = 8 * k + g
+                st[b, z, row : row + 1] = value[:, g * 128 : (g + 1) * 128]
         for peer in zs:
             push(st.at[b, z], st.at[b, z], st_s.at[b * sp_n + z], peer, me)
         push(o_tx.at[b], o_rx.at[z], o_s.at[z], b, me, z != b)
 
+    for b in range(sp_n):
+        st[b, z] = jnp.zeros((24, 128), f32)
     for b in range(sp_n):
         first(b)
         if b < len(c_far):
@@ -598,11 +648,11 @@
         c_far[k].fin()
 
     def stats(b):
-        tops = [st[b, s, 0:1] for s in range(sp_n)]
+        tops = [st[b, s, 0:8] for s in range(sp_n)]
         row_max = functools.reduce(jnp.maximum, tops)
         lifts = [jnp.exp(top - row_max) for top in tops]
-        total = sum(st[b, s, 1:2] * lifts[s] for s in range(sp_n))
-        inner = sum(st[b, s, 2:3] * lifts[s] for s in range(sp_n))
+        total = sum(st[b, s, 8:16] * lifts[s] for s in range(sp_n))
+        inner = sum(st[b, s, 16:24] * lifts[s] for s in range(sp_n))
         return row_max, lifts, total, inner / total
 
     def stats_in(b):
@@ -614,30 +664,21 @@
             pull(o_rx.at[p], o_s.at[p])
         row_max, lifts, total, inner = stats(z)
         o_rx[z] = o_tx[z]
-        mixed = sum(o_rx[s].astype(f32) * lifts[s] for s in range(sp_n))
-        att[z] = (mixed / total).astype(bf16)
-        for peer in zs:
-            push(att.at[z], att.at[z], att_s.at[z], peer, me)
+        mixed = sum(o_rx[s].astype(f32) * line(lifts[s]) for s in range(sp_n))
+        att[z] = (mixed / line(total)).astype(bf16)
 
     def second(i):
         b = z if i == sp_n - 1 else i + (i >= z).astype(jnp.int32)
         if i < sp_n - 1:
             stats_in(b)
         row_max, lifts, total, inner = stats(b)
-        share[0:1] = jnp.exp(st[b, z, 0:1] - row_max) / total
-        share[1:2] = inner
-
-        def body(j, carry):
-            cols = pl.ds(pl.multiple_of(j * tile, tile), tile)
-            prob = p_buf[b, :, cols] * share[0:1, cols]
-            d_score = (prob * (dp_buf[b, :, cols] - share[1:2, cols])).astype(bf16)
-            prob = prob.astype(bf16)
-            dv[...] += nn(prob, dc[b, cols])
-            dk[...] += nn(d_score, qc[b, cols])
-            dq_tx[b, :, cols] = nn(kvt[:HEAD_DIM], d_score).astype(bf16)
-            return carry
-
-        lax.fori_loop(0, steps, body, 0)
+        share = line(jnp.exp(st[b, z, 0:8] - row_max) / total)
+        prob = p_buf[b] * share
+        d_score = (prob * (dp_buf[b] - line(inner))).astype(bf16)
+        prob = prob.astype(bf16)
+        dv[...] += nn(prob, dc[b])
+        dk[...] += nn(d_score, qc[b])
+        dq_tx[b] = nn(kvt[:HEAD_DIM], d_score).astype(bf16)
         if i < sp_n - 1:
             push(dq_tx.at[b], dq_rx.at[z], dq_s.at[z], b, me)
 
@@ -648,6 +689,9 @@
         if i == 0:
             stats_in(z)
             attend()
+        if i == max(0, sp_n - 2):
+            for peer in zs:
+                push(att.at[z], att.at[z], att_s.at[z], peer, me)
 
     for o in range(tp_n):
         part = slice(o * s_loc, (o + 1) * s_loc)
@@ -695,6 +739,8 @@
             piece = att[b, :, h * t_block : (h + 1) * t_block]
             attb[b, h * HEAD_DIM : (h + 1) * HEAD_DIM] = piece
 
+    tile = 256
+
     def weight_grad(j, carry):
         cols = pl.ds(pl.multiple_of(j * tile, tile), tile)
         total = nn(attb[0], cotf[0, :, cols])
@@ -704,6 +750,7 @@
         return carry
 
     lax.fori_loop(0, width // tile, weight_grad, 0)
+    done = [store(2, owg)]
 
     for o in ts:
         pull(g_rx.at[o], g_s.at[o])
@@ -722,18 +769,22 @@
     for i in range(0, s_loc, step):
         part = slice(i, i + step)
         sgrad[part] = norm_back(source[part], sgain[...], un[part])
+    done.append(store(1, sgrad))
 
     mine = ts_tx[me // 2].astype(f32)
     for r in range(3):
         pull(ts_rx.at[r], ts_s.at[r])
     mine = mine + sum(ts_rx[r].astype(f32) for r in range(3))
-    tgrad[...] = cot[...].astype(f32) + norm_back(target[...], tgain[...], mine)
+    tgrad[...] = c_rx[z, me].astype(f32) + norm_back(target[...], tgain[...], mine)
+    done.append(store(0, tgrad))
 
     for one, when in sent:
         if when is None:
             one.wait_send()
         else:
             pl.when(when)(lambda one=one: one.wait_send())
+    for one in done:
+        one.wait()
 
 
 def fused_body(
@@ -760,6 +811,17 @@
     f32, bf16 = jnp.float32, jnp.bfloat16
     vmem, sem = pltpu.VMEM, pltpu.SemaphoreType.DMA
     scratch = [
+        vmem((t_loc, width), bf16),
+        vmem((s_loc, width), bf16),
+        vmem((1, width), f32),
+        vmem((1, width), f32),
+        vmem((width, local_width), bf16),
+        vmem((slab, key_weight.shape[1]), bf16),
+        vmem((slab, key_weight.shape[1]), bf16),
+        vmem((local_width, width), bf16),
+        vmem((t_loc, width), f32),
+        vmem((s_loc, width), f32),
+        vmem((local_width, width), f32),
         vmem((tp_n, t_loc, width), bf16),
         vmem((sp_n, tp_n, t_loc, width), bf16),
         vmem((t_block, width), bf16),
@@ -777,7 +839,7 @@
         vmem((sp_n, lanes, HEAD_DIM), bf16),
         vmem((sp_n, s_block, lanes), f32),
         vmem((sp_n, s_block, lanes), f32),
-        vmem((sp_n, sp_n, 8, lanes), f32),
+        vmem((sp_n, sp_n, 24, 128), f32),
         vmem((sp_n, HEAD_DIM, lanes), bf16),
         vmem((sp_n, HEAD_DIM, lanes), bf16),
         vmem((sp_n, HEAD_DIM, lanes), bf16),
@@ -795,11 +857,11 @@
         vmem((tp_n // 2, t_loc, width), bf16),
         vmem((3, t_loc, width), bf16),
         vmem((s_loc, width), f32),
-        vmem((8, lanes), f32),
         sem((256,)),
         sem((tp_n,)),
         sem((sp_n * tp_n,)),
         sem((pairs * tp_n,)),
+        sem((2 * (sp_n + 1 + pairs),)),
         sem((sp_n,)),
         sem((sp_n,)),
         sem((sp_n,)),
@@ -811,6 +873,8 @@
         sem((tp_n,)),
         sem((tp_n // 2,)),
         sem((3,)),
+        sem((9,)),
+        sem((3,)),
     ]
     return pl.pallas_call(
         functools.partial(fused_kernel, sp_n, tp_n),
@@ -819,8 +883,8 @@
             jax.ShapeDtypeStruct((s_loc, width), f32),
             jax.ShapeDtypeStruct((local_width, width), f32),
         ],
-        in_specs=[pl.BlockSpec(memory_space=pltpu.VMEM)] * 9,
-        out_specs=[pl.BlockSpec(memory_space=pltpu.VMEM)] * 3,
+        in_specs=[pl.BlockSpec(memory_space=pl.ANY)] * 9,
+        out_specs=[pl.BlockSpec(memory_space=pl.ANY)] * 3,
         scratch_shapes=scratch,
         compiler_params=pltpu.CompilerParams(
             collective_id=0,
@@ -843,7 +907,7 @@
 def choose(*args):
     square = lax.axis_size("tp") == 8 and KV_HEADS == 8
     lanes = lax.axis_size("tp") * args[0].shape[0] * args[4].shape[1] // HEAD_DIM
-    if square and lanes % 256 == 0:
+    if square and lanes % 128 == 0 and lanes <= 1024:
         return fused_body(*args)
     return body(*args)
 

time: 102 us -> 93.1 us (0.913)
  the two profiles are of different devices: /device:TPU:19 before, /device:TPU:0 now
where the time goes in v2:
time: 93.1 us; the launch traced here: 92.9 us
  Pallas kernels  86.9 us (93%)
  local copies, waits for them, and re-layouts  5.38 us (6%)
    pallas_call x1, Pallas kernels, fused_body(): pl.pallas_call(functools.partial(fused_kernel, sp_n, tp_n), out_shape=[ja...  86.9 us
    unnamed x5, local copies, waits for them, and re-layouts  5.38 us

profile of v2, /device:TPU:0, one launch (start us, length us, event | category | flops | bytes accessed | tf_op | source)
XLA Modules:
  0.0 92.9 jit_solution(6026753854647980549)
XLA Ops:
  0.6 86.9 %shard_map.112 = (f32[24,2048]{1,0:T(8,128)}, f32[128,2048]{1,0:T(8,128)}, f32[256,2048]{1,0:T(8,128)}) custom-call(bf16[24,2048]{1,0:T(8,128)(2,1)} %refs_0_.1, bf16[128,2048]{1,0:T(8,128)(2,1)} %refs_1_.1, f32[1,2048]{1,0:T(1,128)} %bitcast.2, f32[1,2048]{1,0:T(1,128)} %bitcast.3, bf16[2048,256]{1,0:T(8,128)(2,1)} %refs_4_.1, bf16[256,512]{1,0:T(8,128)(2,1)} %refs_5_.1, ...), custom_call_target="tpu_custom_call" | custom-call | tf_op jit(solution)/shard_map/pallas_call | solution.py:879
  87.5 0.0 copy-start
  87.5 1.8 %copy.15 = f32[24,2048]{1,0:T(8,128)} copy(f32[24,2048]{1,0:T(8,128)} %get-tuple-element.6) | data formatting | bytes 393216
  89.3 2.3 %copy.16 = f32[128,2048]{1,0:T(8,128)} copy(f32[128,2048]{1,0:T(8,128)} %get-tuple-element.7) | data formatting | bytes 2097152
  91.6 0.0 copy-done
  91.6 1.3 %copy.17 = f32[256,2048]{1,0:T(8,128)} copy(f32[256,2048]{1,0:T(8,128)S(1)} %copy-done) | data formatting | bytes 4194304
Async XLA Ops:
  87.5 4.1 %copy-start = (f32[256,2048]{1,0:T(8,128)S(1)}, f32[256,2048]{1,0:T(8,128)}, u32[]{:S(2)}) copy-start(f32[256,2048]{1,0:T(8,128)} %get-tuple-element.8) | copy-start | bytes 6291460

commit v3 on v2

--- a/solution.py
+++ b/solution.py
@@ -380,11 +380,12 @@
     loads, stores = refs[:9], refs[9:12]
     target, source, tgain, sgain, qw, kw, vw, ow = refs[12:20]
     tgrad, sgrad, owg = refs[20:23]
-    (t_rx, c_rx, rows, cotf, w_rx, ns, q_all, d_all, kv_tx, kv_rx, k2, v2, kvt) = refs[23:36]
-    (qc, dc, p_buf, dp_buf, st, o_tx, o_rx, att, attb, dq_tx, dq_rx, qg) = refs[36:48]
-    (dk, dv, g_tx, g_rx, gcat, tt, tp_rx, ts_tx, ts_rx, un) = refs[48:58]
-    send_s, t_s, c_s, w_s, far_s, cz_s, q_s, d_s, kv_s = refs[58:67]
-    st_s, o_s, att_s, dq_s, g_s, tp_s, ts_s, load_s, store_s = refs[67:76]
+    t_rx, c_rx, rows, cotf, w_rx, ns, q_all, d_all, kv_tx, kv_rx = refs[23:33]
+    k2, v2, kvt, qc, dc, p_buf, dp_buf, own, st, st_rx, o_part = refs[33:44]
+    o_tx, o_rx, att, attb, dq_f, dq_tx, dq_rx, qg, dk, dv = refs[44:54]
+    g_tx, g_rx, gcat, tt, tp_rx, ts_tx, ts_rx, un = refs[54:62]
+    send_s, t_s, c_s, w_s, far_s, cz_s, q_s, d_s, kv_s, near_s = refs[62:72]
+    st_s, o_s, att_s, dq_s, g_s, tp_s, ts_s, load_s, store_s = refs[72:81]
     f32, bf16 = jnp.float32, jnp.bfloat16
     z, me = lax.axis_index("sp"), lax.axis_index("tp")
     core = lax.rem(me, 2)
@@ -405,6 +406,7 @@
         return i + 4 - 8 * lax.rem(i // 4, 2)
 
     mate = me + 1 - 2 * core
+    zt, zn = z + 2 - 4 * (z // 2), z + 1 - 2 * lax.rem(z, 2)
     zs = [lax.rem(z + k, sp_n) for k in range(1, sp_n)]
     ts = [lax.rem(me + k, tp_n) for k in range(1, tp_n)]
 
@@ -414,13 +416,26 @@
     for peer in ts:
         pl.semaphore_signal(barrier, inc=1, device_id=(z, peer), device_id_type=MESH)
 
+    for peer in ts:
+        pl.semaphore_signal(barrier, inc=1, device_id=(zn, peer), device_id_type=MESH)
+
     sent = []
+    ring = send_s.shape[0]
+
+    def drain(one, when):
+        if when is None:
+            one.wait_send()
+        else:
+            pl.when(when)(lambda: one.wait_send())
 
     def push(src, dst, sem, zz, i, when=None):
+        turn = len(sent) % ring
+        if len(sent) >= ring:
+            drain(*sent[len(sent) - ring])
         one = pltpu.make_async_remote_copy(
             src_ref=src,
             dst_ref=dst,
-            send_sem=send_s.at[len(sent)],
+            send_sem=send_s.at[turn],
             recv_sem=sem,
             device_id=(zz, i),
             device_id_type=MESH,
@@ -490,7 +505,7 @@
     copies[2].wait()
     t_rx[me] = normalize(target[...], tgain[...])
     copies[8].wait()
-    pl.semaphore_wait(barrier, sp_n - 1 + tp_n - 1)
+    pl.semaphore_wait(barrier, sp_n - 1 + 2 * (tp_n - 1))
 
     some, more = (0, t_loc // 2 // 8 * 8, t_loc), (0, slab // 2, slab)
     t_all = Gather(lambda o: t_rx.at[o], lambda o: t_s.at[o], lambda k: far_s.at[k], some)
@@ -520,16 +535,10 @@
         push(c_rx.at[z, me], c_rx.at[z, me], cz_s.at[z], peer, me)
     copies[5].wait()
     copies[6].wait()
-
-    def weave(c):
-        for j in range(2):
-            head = 2 * c + j
-            cols = slice(head * HEAD_DIM, (head + 1) * HEAD_DIM)
-            both = jnp.concatenate([kw[:, cols], vw[:, cols]], axis=1)
-            w_rx[c, me, :, j * 2 * HEAD_DIM : (j + 1) * 2 * HEAD_DIM] = both
-
+    half = w_rx.shape[3]
     for c in range(pairs):
-        weave(c)
+        part = (kw, vw)[c // 2]
+        w_rx[c, me] = part[:, (c % 2) * half : (c % 2 + 1) * half]
     w_all[0].start()
     copies[1].wait()
     copies[3].wait()
@@ -547,18 +556,18 @@
     for o in range(tp_n):
         rows[o * t_loc : (o + 1) * t_loc] = t_rx[o]
     copies[4].wait()
-    q_all[z] = (nn(rows[...], qw[...]).astype(bf16) * scale).astype(bf16)
-    for peer in zs:
-        push(q_all.at[z], q_all.at[z], q_s.at[z], peer, me)
+    q_all[0] = (nn(rows[...], qw[...]).astype(bf16) * scale).astype(bf16)
+    push(q_all.at[0], q_all.at[1], q_s.at[0], zt, me)
     w_all[1].mid()
     w_all[3].start()
     c_own.rest()
     for o in range(tp_n):
         cotf[z, o * t_loc : (o + 1) * t_loc] = c_rx[z, o]
     copies[7].wait()
-    d_all[z] = nt(cotf[z], ow[...]).astype(bf16)
-    for peer in zs:
-        push(d_all.at[z], d_all.at[z], d_s.at[z], peer, me)
+    d_all[0] = nt(cotf[z], ow[...]).astype(bf16)
+    push(d_all.at[0], d_all.at[1], d_s.at[0], zt, me)
+
+    packed = s_loc // 2
 
     def split_kv(c):
         w_all[c].rest()
@@ -566,43 +575,37 @@
         for o in range(1, tp_n):
             total += nn(ns[:, o * slab : (o + 1) * slab], w_rx[c, o])
         total = total.astype(bf16)
-        for j in range(2):
-            head = 2 * c + j
-            part = total[:, j * 2 * HEAD_DIM : (j + 1) * 2 * HEAD_DIM]
-            kv_tx[head] = part
+        for j in range(tp_n // 2):
+            head = (c % 2) * (tp_n // 2) + j
+            part = total[:, j * HEAD_DIM : (j + 1) * HEAD_DIM]
+            part = jnp.concatenate([part[:packed], part[packed:]], axis=1)
+            kv_tx[c // 2, head] = part
 
             @pl.when(me == head)
             def _():
-                kv_rx[head] = part
-
-            push(kv_tx.at[head], kv_rx.at[me], kv_s.at[me], z, head, me != head)
-
-    w_all[0].fin()
-    split_kv(0)
-    for c in range(2, pairs):
-        w_all[c].mid()
-        w_all[c - 1].fin()
-        split_kv(c - 1)
-    w_all[pairs - 1].fin()
-    split_kv(pairs - 1)
-    for k, p in enumerate(zs):
-        pull(c_rx.at[p, me], cz_s.at[p])
-        c_far[k].start()
-    for p in zs:
-        pull(q_all.at[p], q_s.at[p])
-        pull(d_all.at[p], d_s.at[p])
-    for b in range(sp_n):
-        for h in range(heads):
-            cols = slice(h * HEAD_DIM, (h + 1) * HEAD_DIM)
-            qc[b, h * t_block : (h + 1) * t_block] = q_all[b, :, cols]
-            dc[b, h * t_block : (h + 1) * t_block] = d_all[b, :, cols]
-    for o in ts:
-        pull(kv_rx.at[o], kv_s.at[o])
-    for o in range(tp_n):
-        part = kv_rx[o]
-        k2[o * s_loc : (o + 1) * s_loc] = part[:, :HEAD_DIM]
-        v2[o * s_loc : (o + 1) * s_loc] = part[:, HEAD_DIM:]
-        kvt[:, o * s_loc : (o + 1) * s_loc] = part.astype(f32).T.astype(bf16)
+                kv_rx[0, c // 2, head] = part
+
+            sem = kv_s.at[(c // 2) * tp_n + me]
+            push(kv_tx.at[c // 2, head], kv_rx.at[0, c // 2, me], sem, z, head, me != head)
+            if c // 2 == 1:
+                push(kv_tx.at[1, head], kv_rx.at[1, 1, me], near_s.at[1 + me], zn, head)
+
+    def unpack(w, kind):
+        if w == 0:
+            for o in ts:
+                pull(kv_rx.at[0, kind, o], kv_s.at[kind * tp_n + o])
+            if kind == 0:
+                push(kv_rx.at[0, 0], kv_rx.at[1, 0], near_s.at[0], zn, me)
+        elif kind == 0:
+            pull(kv_rx.at[1, 0], near_s.at[0])
+        else:
+            for o in range(tp_n):
+                pull(kv_rx.at[1, 1, o], near_s.at[1 + o])
+        out = (k2, v2)[kind]
+        for o in range(tp_n):
+            part = kv_rx[w, kind, o]
+            out[w, o * s_loc : o * s_loc + packed] = part[:, :HEAD_DIM]
+            out[w, o * s_loc + packed : (o + 1) * s_loc] = part[:, HEAD_DIM:]
 
     groups = lanes // 128
 
@@ -618,97 +621,142 @@
     def line(x):
         return jnp.concatenate([x[g : g + 1] for g in range(groups)], axis=1)
 
-    def first(b):
-        score = nt(k2[...], qc[b])
+    def take(u, full, sems, out):
+        if u == 1:
+            pull(full.at[1], sems.at[0])
+        for h in range(heads):
+            cols = slice(h * HEAD_DIM, (h + 1) * HEAD_DIM)
+            out[u, h * t_block : (h + 1) * t_block] = full[u, :, cols]
+
+    def weigh(u, w):
+        if w == 0:
+            take(u, q_all, q_s, qc)
+        score = nt(k2[w], qc[u])
         top = fold(jnp.max, score)
         weight = jnp.exp(score - top)
-        d_prob = nt(v2[...], dc[b])
-        total = fold(jnp.sum, weight)
-        inner = fold(jnp.sum, weight * d_prob)
-        p_buf[b] = weight
-        dp_buf[b] = d_prob
-        o_tx[b] = nn(kvt[HEAD_DIM:], weight.astype(bf16)).astype(bf16)
-        for k, value in enumerate((top, total, inner)):
+        own[u, w, 0:1] = top
+        own[u, w, 1:2] = fold(jnp.sum, weight)
+        p_buf[u, w] = weight
+
+    def turn_kv(w):
+        for o in range(tp_n):
+            part = slice(o * s_loc, (o + 1) * s_loc)
+            both = jnp.concatenate([k2[w, part], v2[w, part]], axis=1)
+            kvt[w, :, part] = both.astype(f32).T.astype(bf16)
+
+    def first(u, w):
+        if w == 0:
+            take(u, d_all, d_s, dc)
+        weight = p_buf[u, w]
+        d_prob = nt(v2[w], dc[u])
+        own[u, w, 2:3] = fold(jnp.sum, weight * d_prob)
+        dp_buf[u, w] = d_prob
+        o_part[u, w] = nn(kvt[w, HEAD_DIM:], weight.astype(bf16))
+
+    def join(u):
+        top = jnp.maximum(own[u, 0, 0:1], own[u, 1, 0:1])
+        lifts = [jnp.exp(own[u, w, 0:1] - top) for w in range(2)]
+        total = sum(own[u, w, 1:2] * lifts[w] for w in range(2))
+        inner = sum(own[u, w, 2:3] * lifts[w] for w in range(2)) / total
+        o_tx[u] = (sum(o_part[u, w] * lifts[w] for w in range(2)) / total).astype(bf16)
+        for k, value in enumerate((top + jnp.log(total), inner)):
             for g in range(groups):
-                row = 8 * k + g
-                st[b, z, row : row + 1] = value[:, g * 128 : (g + 1) * 128]
-        for peer in zs:
-            push(st.at[b, z], st.at[b, z], st_s.at[b * sp_n + z], peer, me)
-        push(o_tx.at[b], o_rx.at[z], o_s.at[z], b, me, z != b)
-
-    for b in range(sp_n):
-        st[b, z] = jnp.zeros((24, 128), f32)
-    for b in range(sp_n):
-        first(b)
-        if b < len(c_far):
-            c_far[b].mid()
-        if b >= 1 and b - 1 < len(c_far):
-            c_far[b - 1].fin()
-    for k in range(sp_n - 1, len(c_far)):
-        c_far[k].fin()
-
-    def stats(b):
-        tops = [st[b, s, 0:8] for s in range(sp_n)]
-        row_max = functools.reduce(jnp.maximum, tops)
-        lifts = [jnp.exp(top - row_max) for top in tops]
-        total = sum(st[b, s, 8:16] * lifts[s] for s in range(sp_n))
-        inner = sum(st[b, s, 16:24] * lifts[s] for s in range(sp_n))
-        return row_max, lifts, total, inner / total
-
-    def stats_in(b):
-        for p in zs:
-            pull(st.at[b, p], st_s.at[b * sp_n + p])
+                row = groups * k + g
+                st[u, row : row + 1] = value[:, g * 128 : (g + 1) * 128]
+
+    cut = lanes // 2 // 128 * 128
+    spans = [slice(0, cut), slice(cut, lanes)] if cut else [slice(0, lanes)]
+
+    w_all[0].fin()
+    split_kv(0)
+    w_all[2].mid()
+    w_all[1].fin()
+    split_kv(1)
+    w_all[3].mid()
+    unpack(0, 0)
+    weigh(0, 0)
+    w_all[2].fin()
+    w_all[3].fin()
+    split_kv(2)
+    split_kv(3)
+    for k, p in enumerate(zs):
+        pull(c_rx.at[p, me], cz_s.at[p])
+        c_far[k].start()
+    weigh(1, 0)
+    unpack(1, 0)
+    weigh(0, 1)
+    weigh(1, 1)
+    unpack(0, 1)
+    turn_kv(0)
+    first(0, 0)
+    first(1, 0)
+    unpack(1, 1)
+    turn_kv(1)
+    for u in range(2):
+        first(u, 1)
+        join(u)
+        push(st.at[u], st_rx.at[u], st_s.at[u], zt, me)
+    for n, span in enumerate(spans):
+        push(o_tx.at[1, :, span], o_rx.at[:, span], o_s.at[n], zt, me)
+
+    def stats(u):
+        logs = [st[u, :groups], st_rx[1 - u, :groups]]
+        inners = [st[u, groups:], st_rx[1 - u, groups:]]
+        top = jnp.maximum(*logs)
+        log_total = top + jnp.log(sum(jnp.exp(x - top) for x in logs))
+        lifts = [jnp.exp(x - log_total) for x in logs]
+        return log_total, lifts, inners[0] * lifts[0] + inners[1] * lifts[1]
 
     def attend():
-        for p in zs:
-            pull(o_rx.at[p], o_s.at[p])
-        row_max, lifts, total, inner = stats(z)
-        o_rx[z] = o_tx[z]
-        mixed = sum(o_rx[s].astype(f32) * line(lifts[s]) for s in range(sp_n))
-        att[z] = (mixed / line(total)).astype(bf16)
-
-    def second(i):
-        b = z if i == sp_n - 1 else i + (i >= z).astype(jnp.int32)
-        if i < sp_n - 1:
-            stats_in(b)
-        row_max, lifts, total, inner = stats(b)
-        share = line(jnp.exp(st[b, z, 0:8] - row_max) / total)
-        prob = p_buf[b] * share
-        d_score = (prob * (dp_buf[b] - line(inner))).astype(bf16)
+        lifts = [line(x) for x in stats(0)[1]]
+        for n, span in enumerate(spans):
+            pull(o_rx.at[:, span], o_s.at[n])
+            mine = o_tx[0, :, span].astype(f32) * lifts[0][:, span]
+            other = o_rx[:, span].astype(f32) * lifts[1][:, span]
+            att[z, :, span] = (mine + other).astype(bf16)
+            for peer in zs:
+                part = att.at[z, :, span]
+                push(part, part, att_s.at[n * sp_n + z], peer, me)
+
+    def second(u, w, start):
+        log_total, lifts, inner = stats(u)
+        prob = p_buf[u, w] * jnp.exp(own[u, w, 0:1] - line(log_total))
+        d_score = (prob * (dp_buf[u, w] - line(inner))).astype(bf16)
         prob = prob.astype(bf16)
-        dv[...] += nn(prob, dc[b])
-        dk[...] += nn(d_score, qc[b])
-        dq_tx[b] = nn(kvt[:HEAD_DIM], d_score).astype(bf16)
-        if i < sp_n - 1:
-            push(dq_tx.at[b], dq_rx.at[z], dq_s.at[z], b, me)
-
-    dk[...] = jnp.zeros_like(dk)
-    dv[...] = jnp.zeros_like(dv)
-    for i in range(sp_n):
-        second(i)
-        if i == 0:
-            stats_in(z)
-            attend()
-        if i == max(0, sp_n - 2):
-            for peer in zs:
-                push(att.at[z], att.at[z], att_s.at[z], peer, me)
-
-    for o in range(tp_n):
-        part = slice(o * s_loc, (o + 1) * s_loc)
-        g_tx[o] = jnp.concatenate([dk[part], dv[part]], axis=1).astype(bf16)
-    for o in ts:
-        push(g_tx.at[o], g_rx.at[me], g_s.at[me], z, o)
-    g_rx[me] = g_tx[me]
-
-    for p in zs:
-        pull(dq_rx.at[p], dq_s.at[p])
-    dq_rx[z] = dq_tx[z]
-    summed = sum(dq_rx[s].astype(f32) for s in range(sp_n)) * scale
+        d_value, d_key = nn(prob, dc[u]), nn(d_score, qc[u])
+        dv[w] = d_value if u == 1 else dv[w] + d_value
+        dk[w] = d_key if u == 1 else dk[w] + d_key
+        d_query = nn(kvt[w, :HEAD_DIM], d_score)
+        dq_f[u] = d_query if start else dq_f[u] + d_query
+
+    def send_g(w, plane):
+        for o in range(tp_n):
+            part = slice(o * s_loc, (o + 1) * s_loc)
+            g_tx[w, o] = jnp.concatenate([dk[w, part], dv[w, part]], axis=1).astype(bf16)
+        for o in ts + ([me] if w == 1 else []):
+            push(g_tx.at[w, o], g_rx.at[w, me], g_s.at[w * tp_n + me], plane, o)
+
+    pull(st_rx.at[0], st_s.at[0])
+    second(1, 0, True)
+    second(1, 1, False)
+    dq_tx[...] = dq_f[1].astype(bf16)
+    push(dq_tx, dq_rx, dq_s.at[0], zt, me)
+    pull(st_rx.at[1], st_s.at[1])
+    second(0, 1, True)
+    send_g(1, zn)
+    c_far[0].mid()
+    c_far[1].mid()
+    second(0, 0, False)
+    send_g(0, z)
+    g_rx[0, me] = g_tx[0, me]
+    c_far[2].mid()
+    pull(dq_rx, dq_s.at[0])
+    attend()
+    summed = (dq_f[0] + dq_rx[...].astype(f32)) * scale
     summed = summed.T
     for h in range(heads):
         piece = summed[h * t_block : (h + 1) * t_block].astype(bf16)
         qg[:, h * HEAD_DIM : (h + 1) * HEAD_DIM] = piece
-
     wide = 512
 
     def terms(j, carry):
@@ -722,40 +770,23 @@
     chips = tp_n // 2
     for c in range(chips):
         push(tt.at[2 * c + 1 - core], tp_rx.at[c], tp_s.at[c], z, mate)
+    tile = 256
+
     for c in range(chips):
         pull(tp_rx.at[c], tp_s.at[c])
         ts_tx[c] = (tt[2 * c + core].astype(f32) + tp_rx[c].astype(f32)).astype(bf16)
     for r, peer in enumerate((across(along(me)), across(me), along(me))):
         push(ts_tx.at[peer // 2], ts_rx.at[r], ts_s.at[r], z, peer)
-
-    for k, p in enumerate(zs):
-        c_far[k].rest()
-        for o in range(tp_n):
-            cotf[p, o * t_loc : (o + 1) * t_loc] = c_rx[p, o]
-    for p in zs:
-        pull(att.at[p], att_s.at[p])
-    for b in range(sp_n):
-        for h in range(heads):
-            piece = att[b, :, h * t_block : (h + 1) * t_block]
-            attb[b, h * HEAD_DIM : (h + 1) * HEAD_DIM] = piece
-
-    tile = 256
-
-    def weight_grad(j, carry):
-        cols = pl.ds(pl.multiple_of(j * tile, tile), tile)
-        total = nn(attb[0], cotf[0, :, cols])
-        for b in range(1, sp_n):
-            total += nn(attb[b], cotf[b, :, cols])
-        owg[:, cols] = total
-        return carry
-
-    lax.fori_loop(0, width // tile, weight_grad, 0)
-    done = [store(2, owg)]
-
+    for item in c_far:
+        item.fin()
+    side = tp_n * HEAD_DIM
     for o in ts:
-        pull(g_rx.at[o], g_s.at[o])
+        pull(g_rx.at[0, o], g_s.at[o])
     for o in range(tp_n):
-        gcat[:, o * 2 * HEAD_DIM : (o + 1) * 2 * HEAD_DIM] = g_rx[o]
+        pull(g_rx.at[1, o], g_s.at[tp_n + o])
+        part = (g_rx[0, o].astype(f32) + g_rx[1, o].astype(f32)).astype(bf16)
+        gcat[:, o * HEAD_DIM : (o + 1) * HEAD_DIM] = part[:, :HEAD_DIM]
+        gcat[:, side + o * HEAD_DIM : side + (o + 1) * HEAD_DIM] = part[:, HEAD_DIM:]
 
     def upstream(o, carry):
         cols = pl.ds(pl.multiple_of(o * slab, slab), slab)
@@ -769,8 +800,31 @@
     for i in range(0, s_loc, step):
         part = slice(i, i + step)
         sgrad[part] = norm_back(source[part], sgain[...], un[part])
-    done.append(store(1, sgrad))
-
+    done = [store(1, sgrad)]
+    for k, p in enumerate(zs):
+        c_far[k].rest()
+        for o in range(tp_n):
+            cotf[p, o * t_loc : (o + 1) * t_loc] = c_rx[p, o]
+    for p in zs:
+        for n, span in enumerate(spans):
+            pull(att.at[p, :, span], att_s.at[n * sp_n + p])
+    for b in range(sp_n):
+        for h in range(heads):
+            piece = att[b, :, h * t_block : (h + 1) * t_block]
+            attb[b, h * HEAD_DIM : (h + 1) * HEAD_DIM] = piece
+
+    def weight_grad(j, carry):
+        cols = pl.ds(pl.multiple_of(j * tile, tile), tile)
+        owg[:, cols] = sum(nn(attb[b], cotf[b, :, cols]) for b in range(sp_n))
+        return carry
+
+    rest = width // tile // 2
+    for n in range(2):
+        lax.fori_loop(n * rest, (n + 1) * rest, weight_grad, 0)
+        part = slice(n * rest * tile, (n + 1) * rest * tile)
+        one = pltpu.make_async_copy(owg.at[:, part], stores[2].at[:, part], store_s.at[2 + n])
+        one.start()
+        done.append(one)
     mine = ts_tx[me // 2].astype(f32)
     for r in range(3):
         pull(ts_rx.at[r], ts_s.at[r])
@@ -778,13 +832,41 @@
     tgrad[...] = c_rx[z, me].astype(f32) + norm_back(target[...], tgain[...], mine)
     done.append(store(0, tgrad))
 
-    for one, when in sent:
-        if when is None:
-            one.wait_send()
-        else:
-            pl.when(when)(lambda one=one: one.wait_send())
+    for one, when in sent[-ring:]:
+        drain(one, when)
     for one in done:
         one.wait()
+
+
+def finish_kernel(*refs):
+    ins, outs, held = refs[:3], refs[3:6], refs[6:9]
+    in_sems, out_sems = refs[9:11]
+    pieces = []
+    for i in (2, 1, 0):
+        size = ins[i].shape[0]
+        step = max(size // 4 // 8 * 8, 8)
+        for at in range(0, size, step):
+            part = pl.ds(at, min(step, size - at))
+            pieces.append((ins[i].at[part], held[i].at[part], outs[i].at[part]))
+    for k, (a, b, c) in enumerate(pieces):
+        pltpu.make_async_copy(a, b, in_sems.at[k]).start()
+    for k, (a, b, c) in enumerate(pieces):
+        pltpu.make_async_copy(a, b, in_sems.at[k]).wait()
+        pltpu.make_async_copy(b, c, out_sems.at[k]).start()
+    for k, (a, b, c) in enumerate(pieces):
+        pltpu.make_async_copy(b, c, out_sems.at[k]).wait()
+
+
+def finish(*arrays):
+    return pl.pallas_call(
+        finish_kernel,
+        out_shape=[jax.ShapeDtypeStruct(a.shape, a.dtype) for a in arrays],
+        in_specs=[pl.BlockSpec(memory_space=pltpu.HBM)] * 3,
+        out_specs=[pl.BlockSpec(memory_space=pl.ANY)] * 3,
+        scratch_shapes=[pltpu.VMEM(a.shape, a.dtype) for a in arrays]
+        + [pltpu.SemaphoreType.DMA((12,)), pltpu.SemaphoreType.DMA((12,))],
+        compiler_params=pltpu.CompilerParams(vmem_limit_bytes=67043328),
+    )(*arrays)
 
 
 def fused_body(
@@ -810,6 +892,7 @@
     two = 2 * HEAD_DIM
     f32, bf16 = jnp.float32, jnp.bfloat16
     vmem, sem = pltpu.VMEM, pltpu.SemaphoreType.DMA
+    sends = 48
     scratch = [
         vmem((t_loc, width), bf16),
         vmem((s_loc, width), bf16),
@@ -828,55 +911,60 @@
         vmem((sp_n, t_block, width), bf16),
         vmem((pairs, tp_n, slab, 2 * two), bf16),
         vmem((s_loc, width), bf16),
-        vmem((sp_n, t_block, local_width), bf16),
-        vmem((sp_n, t_block, local_width), bf16),
-        vmem((tp_n, s_loc, two), bf16),
-        vmem((tp_n, s_loc, two), bf16),
-        vmem((s_block, HEAD_DIM), bf16),
-        vmem((s_block, HEAD_DIM), bf16),
-        vmem((two, s_block), bf16),
-        vmem((sp_n, lanes, HEAD_DIM), bf16),
-        vmem((sp_n, lanes, HEAD_DIM), bf16),
-        vmem((sp_n, s_block, lanes), f32),
-        vmem((sp_n, s_block, lanes), f32),
-        vmem((sp_n, sp_n, 24, 128), f32),
-        vmem((sp_n, HEAD_DIM, lanes), bf16),
-        vmem((sp_n, HEAD_DIM, lanes), bf16),
+        vmem((2, t_block, local_width), bf16),
+        vmem((2, t_block, local_width), bf16),
+        vmem((2, tp_n, s_loc // 2, two), bf16),
+        vmem((2, 2, tp_n, s_loc // 2, two), bf16),
+        vmem((2, s_block, HEAD_DIM), bf16),
+        vmem((2, s_block, HEAD_DIM), bf16),
+        vmem((2, two, s_block), bf16),
+        vmem((2, lanes, HEAD_DIM), bf16),
+        vmem((2, lanes, HEAD_DIM), bf16),
+        vmem((2, 2, s_block, lanes), f32),
+        vmem((2, 2, s_block, lanes), f32),
+        vmem((2, 2, 3, lanes), f32),
+        vmem((2, lanes // 64, 128), f32),
+        vmem((2, lanes // 64, 128), f32),
+        vmem((2, 2, HEAD_DIM, lanes), f32),
+        vmem((2, HEAD_DIM, lanes), bf16),
+        vmem((HEAD_DIM, lanes), bf16),
         vmem((sp_n, HEAD_DIM, lanes), bf16),
         vmem((sp_n, local_width, t_block), bf16),
-        vmem((sp_n, HEAD_DIM, lanes), bf16),
-        vmem((sp_n, HEAD_DIM, lanes), bf16),
+        vmem((2, HEAD_DIM, lanes), f32),
+        vmem((HEAD_DIM, lanes), bf16),
+        vmem((HEAD_DIM, lanes), bf16),
         vmem((t_block, local_width), bf16),
-        vmem((s_block, HEAD_DIM), f32),
-        vmem((s_block, HEAD_DIM), f32),
-        vmem((tp_n, s_loc, two), bf16),
-        vmem((tp_n, s_loc, two), bf16),
+        vmem((2, s_block, HEAD_DIM), f32),
+        vmem((2, s_block, HEAD_DIM), f32),
+        vmem((2, tp_n, s_loc, two), bf16),
+        vmem((2, tp_n, s_loc, two), bf16),
         vmem((s_loc, tp_n * two), bf16),
         vmem((tp_n, t_loc, width), bf16),
         vmem((tp_n // 2, t_loc, width), bf16),
         vmem((tp_n // 2, t_loc, width), bf16),
         vmem((3, t_loc, width), bf16),
         vmem((s_loc, width), f32),
-        sem((256,)),
+        sem((sends,)),
         sem((tp_n,)),
         sem((sp_n * tp_n,)),
         sem((pairs * tp_n,)),
         sem((2 * (sp_n + 1 + pairs),)),
         sem((sp_n,)),
-        sem((sp_n,)),
-        sem((sp_n,)),
-        sem((tp_n,)),
-        sem((sp_n * sp_n,)),
-        sem((sp_n,)),
-        sem((sp_n,)),
-        sem((sp_n,)),
-        sem((tp_n,)),
+        sem((1,)),
+        sem((1,)),
+        sem((2 * tp_n,)),
+        sem((1 + tp_n,)),
+        sem((2,)),
+        sem((2,)),
+        sem((2 * sp_n,)),
+        sem((1,)),
+        sem((2 * tp_n,)),
         sem((tp_n // 2,)),
         sem((3,)),
         sem((9,)),
-        sem((3,)),
+        sem((4,)),
     ]
-    return pl.pallas_call(
+    results = pl.pallas_call(
         functools.partial(fused_kernel, sp_n, tp_n),
         out_shape=[
             jax.ShapeDtypeStruct((t_loc, width), f32),
@@ -902,10 +990,11 @@
         out_weight,
         out_cotangent,
     )
+    return tuple(finish(*results))
 
 
 def choose(*args):
-    square = lax.axis_size("tp") == 8 and KV_HEADS == 8
+    square = lax.axis_size("tp") == 8 and KV_HEADS == 8 and lax.axis_size("sp") == 4
     lanes = lax.axis_size("tp") * args[0].shape[0] * args[4].shape[1] // HEAD_DIM
     if square and lanes % 128 == 0 and lanes <= 1024:
         return fused_body(*args)

time: 93.1 us -> 76.3 us (0.82)
  Pallas kernels: 86.9 us -> 75.4 us
  local copies, waits for them, and re-layouts: 5.38 us -> 0 us
    pallas_call x1, Pallas kernels: 86.9 us -> 72.4 us  [fused_body(): pl.pallas_call(functools.partial(fused_kernel, sp_n, tp_n), out_shape=[ja...]
    unnamed x5 -> x0, local copies, waits for them, and re-layouts: 5.38 us -> none
    pallas_call x0 -> x1, Pallas kernels: none -> 2.96 us  [finish(): pl.pallas_call(finish_kernel, out_shape=[jax.ShapeDtypeStruct(a.shape, a....]
where the time goes in v3:
time: 76.3 us; the launch traced here: 76.2 us
  Pallas kernels  75.4 us (99%)
  between operations  0.82 us (1%)
    pallas_call x1, Pallas kernels, fused_body(): pl.pallas_call(functools.partial(fused_kernel, sp_n, tp_n), out_shape=[ja...  72.4 us
    pallas_call x1, Pallas kernels, finish(): pl.pallas_call(finish_kernel, out_shape=[jax.ShapeDtypeStruct(a.shape, a....  2.96 us

profile of v3, /device:TPU:0, one launch (start us, length us, event | category | flops | bytes accessed | tf_op | source)
XLA Modules:
  0.0 76.2 jit_solution(1202145262549082089)
XLA Ops:
  0.6 72.4 %shard_map.112 = (f32[24,2048]{1,0:T(8,128)}, f32[128,2048]{1,0:T(8,128)}, f32[256,2048]{1,0:T(8,128)}) custom-call(bf16[24,2048]{1,0:T(8,128)(2,1)} %refs_0_.1, bf16[128,2048]{1,0:T(8,128)(2,1)} %refs_1_.1, f32[1,2048]{1,0:T(1,128)} %bitcast.2, f32[1,2048]{1,0:T(1,128)} %bitcast.3, bf16[2048,256]{1,0:T(8,128)(2,1)} %refs_4_.1, bf16[256,512]{1,0:T(8,128)(2,1)} %refs_5_.1, ...), custom_call_target="tpu_custom_call" | custom-call | tf_op jit(solution)/shard_map/pallas_call | solution.py:967
  73.0 3.0 %shard_map.113 = (f32[24,2048]{1,0:T(8,128)}, f32[128,2048]{1,0:T(8,128)}, f32[256,2048]{1,0:T(8,128)}) custom-call(f32[24,2048]{1,0:T(8,128)} %get-tuple-element.6.refs_0_, f32[128,2048]{1,0:T(8,128)} %get-tuple-element.7.refs_1_, f32[256,2048]{1,0:T(8,128)} %get-tuple-element.8.refs_2_), custom_call_target="tpu_custom_call" | custom-call | tf_op jit(solution)/shard_map/pallas_call | solution.py:861

commit v4 on v3

--- a/solution.py
+++ b/solution.py
@@ -530,7 +530,6 @@
     ]
 
     t_all.start()
-    c_own.start()
     for peer in zs:
         push(c_rx.at[z, me], c_rx.at[z, me], cz_s.at[z], peer, me)
     copies[5].wait()
@@ -545,13 +544,11 @@
     step = min(s_loc, 32)
     for i in range(0, s_loc, step):
         ns[i : i + step] = normalize(source[i : i + step], sgain[...])
+    w_all[1].start()
     t_all.mid()
-    c_own.mid()
-    w_all[1].start()
     w_all[0].mid()
     w_all[2].start()
     t_all.fin()
-    c_own.fin()
     t_all.rest()
     for o in range(tp_n):
         rows[o * t_loc : (o + 1) * t_loc] = t_rx[o]
@@ -560,12 +557,6 @@
     push(q_all.at[0], q_all.at[1], q_s.at[0], zt, me)
     w_all[1].mid()
     w_all[3].start()
-    c_own.rest()
-    for o in range(tp_n):
-        cotf[z, o * t_loc : (o + 1) * t_loc] = c_rx[z, o]
-    copies[7].wait()
-    d_all[0] = nt(cotf[z], ow[...]).astype(bf16)
-    push(d_all.at[0], d_all.at[1], d_s.at[0], zt, me)
 
     packed = s_loc // 2
 
@@ -670,15 +661,24 @@
     w_all[0].fin()
     split_kv(0)
     w_all[2].mid()
+    c_own.start()
     w_all[1].fin()
     split_kv(1)
     w_all[3].mid()
+    w_all[2].fin()
     unpack(0, 0)
+    c_own.mid()
     weigh(0, 0)
-    w_all[2].fin()
     w_all[3].fin()
     split_kv(2)
     split_kv(3)
+    c_own.fin()
+    c_own.rest()
+    for o in range(tp_n):
+        cotf[z, o * t_loc : (o + 1) * t_loc] = c_rx[z, o]
+    copies[7].wait()
+    d_all[0] = nt(cotf[z], ow[...]).astype(bf16)
+    push(d_all.at[0], d_all.at[1], d_s.at[0], zt, me)
     for k, p in enumerate(zs):
         pull(c_rx.at[p, me], cz_s.at[p])
         c_far[k].start()
@@ -689,13 +689,16 @@
     unpack(0, 1)
     turn_kv(0)
     first(0, 0)
-    first(1, 0)
     unpack(1, 1)
     turn_kv(1)
-    for u in range(2):
-        first(u, 1)
-        join(u)
-        push(st.at[u], st_rx.at[u], st_s.at[u], zt, me)
+    first(0, 1)
+    join(0)
+    push(st.at[0], st_rx.at[0], st_s.at[0], zt, me)
+    c_far[0].mid()
+    first(1, 0)
+    first(1, 1)
+    join(1)
+    push(st.at[1], st_rx.at[1], st_s.at[1], zt, me)
     for n, span in enumerate(spans):
         push(o_tx.at[1, :, span], o_rx.at[:, span], o_s.at[n], zt, me)
 
@@ -736,22 +739,20 @@
         for o in ts + ([me] if w == 1 else []):
             push(g_tx.at[w, o], g_rx.at[w, me], g_s.at[w * tp_n + me], plane, o)
 
+    c_far[1].mid()
     pull(st_rx.at[0], st_s.at[0])
     second(1, 0, True)
+    c_far[2].mid()
     second(1, 1, False)
     dq_tx[...] = dq_f[1].astype(bf16)
     push(dq_tx, dq_rx, dq_s.at[0], zt, me)
     pull(st_rx.at[1], st_s.at[1])
     second(0, 1, True)
     send_g(1, zn)
-    c_far[0].mid()
-    c_far[1].mid()
     second(0, 0, False)
     send_g(0, z)
     g_rx[0, me] = g_tx[0, me]
-    c_far[2].mid()
     pull(dq_rx, dq_s.at[0])
-    attend()
     summed = (dq_f[0] + dq_rx[...].astype(f32)) * scale
     summed = summed.T
     for h in range(heads):
@@ -770,6 +771,7 @@
     chips = tp_n // 2
     for c in range(chips):
         push(tt.at[2 * c + 1 - core], tp_rx.at[c], tp_s.at[c], z, mate)
+    attend()
     tile = 256
 
     for c in range(chips):
@@ -818,8 +820,8 @@
         owg[:, cols] = sum(nn(attb[b], cotf[b, :, cols]) for b in range(sp_n))
         return carry
 
-    rest = width // tile // 2
-    for n in range(2):
+    rest = width // tile // 4
+    for n in range(4):
         lax.fori_loop(n * rest, (n + 1) * rest, weight_grad, 0)
         part = slice(n * rest * tile, (n + 1) * rest * tile)
         one = pltpu.make_async_copy(owg.at[:, part], stores[2].at[:, part], store_s.at[2 + n])
@@ -962,7 +964,7 @@
         sem((tp_n // 2,)),
         sem((3,)),
         sem((9,)),
-        sem((4,)),
+        sem((6,)),
     ]
     results = pl.pallas_call(
         functools.partial(fused_kernel, sp_n, tp_n),

time: 76.3 us -> 75.7 us (level)
  no operation moved by 1% of the time
where the time goes in v4:
time: 75.7 us; the launch traced here: 75.6 us
  Pallas kernels  74.7 us (99%)
  between operations  0.82 us (1%)
    pallas_call x1, Pallas kernels, fused_body(): pl.pallas_call(functools.partial(fused_kernel, sp_n, tp_n), out_shape=[ja...  71.8 us
    pallas_call x1, Pallas kernels, finish(): pl.pallas_call(finish_kernel, out_shape=[jax.ShapeDtypeStruct(a.shape, a....  2.96 us

profile of v4, /device:TPU:0, one launch (start us, length us, event | category | flops | bytes accessed | tf_op | source)
XLA Modules:
  0.0 75.6 jit_solution(13244957533297863159)
XLA Ops:
  0.6 71.8 %shard_map.112 = (f32[24,2048]{1,0:T(8,128)}, f32[128,2048]{1,0:T(8,128)}, f32[256,2048]{1,0:T(8,128)}) custom-call(bf16[24,2048]{1,0:T(8,128)(2,1)} %refs_0_.1, bf16[128,2048]{1,0:T(8,128)(2,1)} %refs_1_.1, f32[1,2048]{1,0:T(1,128)} %bitcast.2, f32[1,2048]{1,0:T(1,128)} %bitcast.3, bf16[2048,256]{1,0:T(8,128)(2,1)} %refs_4_.1, bf16[256,512]{1,0:T(8,128)(2,1)} %refs_5_.1, ...), custom_call_target="tpu_custom_call" | custom-call | tf_op jit(solution)/shard_map/pallas_call | solution.py:969
  72.4 3.0 %shard_map.113 = (f32[24,2048]{1,0:T(8,128)}, f32[128,2048]{1,0:T(8,128)}, f32[256,2048]{1,0:T(8,128)}) custom-call(f32[24,2048]{1,0:T(8,128)} %get-tuple-element.6.refs_0_, f32[128,2048]{1,0:T(8,128)} %get-tuple-element.7.refs_1_, f32[256,2048]{1,0:T(8,128)} %get-tuple-element.8.refs_2_), custom_call_target="tpu_custom_call" | custom-call | tf_op jit(solution)/shard_map/pallas_call | solution.py:863

commit v5 on v4

--- a/solution.py
+++ b/solution.py
@@ -761,13 +761,14 @@
     wide = 512
 
     def terms(j, carry):
-        cols = pl.ds(pl.multiple_of(j * wide, wide), wide)
+        cols = pl.ds(j * wide, wide)
         value = nt(qg[...], qw[cols])
         for o in range(tp_n):
             tt[o, :, cols] = value[o * t_loc : (o + 1) * t_loc].astype(bf16)
         return carry
 
-    lax.fori_loop(0, width // wide, terms, 0)
+    for j in range(width // wide):
+        terms(j, 0)
     chips = tp_n // 2
     for c in range(chips):
         push(tt.at[2 * c + 1 - core], tp_rx.at[c], tp_s.at[c], z, mate)
@@ -791,14 +792,16 @@
         gcat[:, side + o * HEAD_DIM : side + (o + 1) * HEAD_DIM] = part[:, HEAD_DIM:]
 
     def upstream(o, carry):
-        cols = pl.ds(pl.multiple_of(o * slab, slab), slab)
-        total = nt(gcat[:, : 4 * HEAD_DIM], w_rx[0, o])
-        for c in range(1, pairs):
-            total += nt(gcat[:, c * 4 * HEAD_DIM : (c + 1) * 4 * HEAD_DIM], w_rx[c, o])
-        un[:, cols] = total
+        for n in range(2):
+            at = 2 * o + n
+            cols = pl.ds(pl.multiple_of(at * slab, slab), slab)
+            total = nt(gcat[:, : 4 * HEAD_DIM], w_rx[0, at])
+            for c in range(1, pairs):
+                total += nt(gcat[:, c * 4 * HEAD_DIM : (c + 1) * 4 * HEAD_DIM], w_rx[c, at])
+            un[:, cols] = total
         return carry
 
-    lax.fori_loop(0, tp_n, upstream, 0)
+    lax.fori_loop(0, tp_n // 2, upstream, 0)
     for i in range(0, s_loc, step):
         part = slice(i, i + step)
         sgrad[part] = norm_back(source[part], sgain[...], un[part])
@@ -816,13 +819,14 @@
             attb[b, h * HEAD_DIM : (h + 1) * HEAD_DIM] = piece
 
     def weight_grad(j, carry):
-        cols = pl.ds(pl.multiple_of(j * tile, tile), tile)
+        cols = pl.ds(j * tile, tile)
         owg[:, cols] = sum(nn(attb[b], cotf[b, :, cols]) for b in range(sp_n))
         return carry
 
     rest = width // tile // 4
     for n in range(4):
-        lax.fori_loop(n * rest, (n + 1) * rest, weight_grad, 0)
+        for j in range(n * rest, (n + 1) * rest):
+            weight_grad(j, 0)
         part = slice(n * rest * tile, (n + 1) * rest * tile)
         one = pltpu.make_async_copy(owg.at[:, part], stores[2].at[:, part], store_s.at[2 + n])
         one.start()

time: 75.7 us -> 74 us (0.978)
  Pallas kernels: 74.7 us -> 73 us
    pallas_call x1, Pallas kernels: 71.8 us -> 70 us  [fused_body(): pl.pallas_call(functools.partial(fused_kernel, sp_n, tp_n), out_shape=[ja...]
where the time goes in v5:
time: 74 us; the launch traced here: 73.8 us
  Pallas kernels  73 us (99%)
  between operations  0.82 us (1%)
    pallas_call x1, Pallas kernels, fused_body(): pl.pallas_call(functools.partial(fused_kernel, sp_n, tp_n), out_shape=[ja...  70 us
    pallas_call x1, Pallas kernels, finish(): pl.pallas_call(finish_kernel, out_shape=[jax.ShapeDtypeStruct(a.shape, a....  2.96 us

profile of v5, /device:TPU:0, one launch (start us, length us, event | category | flops | bytes accessed | tf_op | source)
XLA Modules:
  0.0 73.8 jit_solution(16508207163638370622)
XLA Ops:
  0.6 70.0 %shard_map.112 = (f32[24,2048]{1,0:T(8,128)}, f32[128,2048]{1,0:T(8,128)}, f32[256,2048]{1,0:T(8,128)}) custom-call(bf16[24,2048]{1,0:T(8,128)(2,1)} %refs_0_.1, bf16[128,2048]{1,0:T(8,128)(2,1)} %refs_1_.1, f32[1,2048]{1,0:T(1,128)} %bitcast.2, f32[1,2048]{1,0:T(1,128)} %bitcast.3, bf16[2048,256]{1,0:T(8,128)(2,1)} %refs_4_.1, bf16[256,512]{1,0:T(8,128)(2,1)} %refs_5_.1, ...), custom_call_target="tpu_custom_call" | custom-call | tf_op jit(solution)/shard_map/pallas_call | solution.py:973
  70.7 3.0 %shard_map.113 = (f32[24,2048]{1,0:T(8,128)}, f32[128,2048]{1,0:T(8,128)}, f32[256,2048]{1,0:T(8,128)}) custom-call(f32[24,2048]{1,0:T(8,128)} %get-tuple-element.6.refs_0_, f32[128,2048]{1,0:T(8,128)} %get-tuple-element.7.refs_1_, f32[256,2048]{1,0:T(8,128)} %get-tuple-element.8.refs_2_), custom_call_target="tpu_custom_call" | custom-call | tf_op jit(solution)/shard_map/pallas_call | solution.py:867
